TPU v7x, 32 devices: a whole 2x2x4 slice. The times are simulated.
32 devices in a mesh: sp: 4 (over y, x), tp: 8 (over z, core).
Axes of the slice: x: 2, y: 2, z: 4, core: 2. Of those that a mesh axis runs over, the one named last changes fastest.
Arguments:
- layer_in: bfloat16 [1280, 2048], P('sp', 'tp'), may hold values from -6 to 6
- out_cot: bfloat16 [1280, 2048], P('sp', 'tp'), may hold values from -6 to 6
- route_ids: int32 [1280, 2], P('sp'), may hold values from 0 to 3, all different within a row; in each aligned block of 320 rows (0 to 319, 320 to 639, ...) at most 320 rows name the same one
- route_probs: float32 [1280, 2], P('sp'), may hold values from 0.2 to 1
- group_prob: float32 [1280], P('sp'), may hold values from 0.3 to 1
- gate_weight: bfloat16 [4, 2048, 2048], P('sp', 'tp'), may hold values from -0.125 to 0.125
- up_weight: bfloat16 [4, 2048, 2048], P('sp', 'tp'), may hold values from -0.125 to 0.125
- down_weight: bfloat16 [4, 2048, 2048], P('sp', 'tp'), may hold values from -0.125 to 0.125
- out_weight: bfloat16 [2048, 2048], P(None, 'tp'), may hold values from -0.125 to 0.125
- query: bfloat16 [1280, 1024], P('sp', 'tp'), may hold values from -6 to 6
- key_in: bfloat16 [1280, 1024], P('sp', 'tp'), may hold values from -0.75 to 0.75
- value: bfloat16 [1280, 2048], P('sp', 'tp'), may hold values from -6 to 6
- decay_logit: bfloat16 [1280, 1024], P('sp', 'tp'), may hold values from -2.5 to 8.5, as said below
Outputs:
- gate_grad: float32 [4, 2048, 2048], P('sp', 'tp')
- up_grad: float32 [4, 2048, 2048], P('sp', 'tp')
- down_grad: float32 [4, 2048, 2048], P('sp', 'tp')
- proj_grad: float32 [2048, 2048], P('sp', 'tp')
- query_grad: float32 [1280, 1024], P('sp', 'tp')
- key_grad: float32 [1280, 1024], P('sp', 'tp')
- value_grad: float32 [1280, 2048], P('sp', 'tp')
- logit_grad: float32 [1280, 1024], P('sp', 'tp')
Inputs may be any that keep to these rules, and one draw needn't show every extreme that they name: `route_ids`: each row names two different experts of 0 to 3; every expert is named by some row; within each aligned block of 320 rows (the rows of one device) no expert is named more than 320 times, and in some block one expert is named exactly 320 times. `decay_logit`: values lie between -2.5 and 8.5; even heads have pre-activations near 5, odd heads near 1.
All inputs are finite; a program needn't handle non-finite values.
Results may differ from a plain program's by a relative error of at most 0.019.
Values may be sent and summed in bfloat16 or wider, within the bound.
A program may use at most 128 MiB of HBM per device.

v0:
```python
import functools
import jax
import jax.numpy as jnp
from jax import lax
from jax.experimental import pallas as pl
from jax.experimental.pallas import tpu as pltpu
from jax.sharding import PartitionSpec as P

DK = 64
DV = 128
BLOCK = 64


decay_temp = 16.0
highest = lax.Precision.HIGH


def prefix(x, axis, join, neutral, backward):
    count = lax.axis_size(axis)
    place = lax.axis_index(axis)
    ahead = count - 1 - place if backward else place
    gathered = jax.tree.map(
        lambda a, kind: lax.all_gather(a.astype(kind), axis),
        x,
        jax.tree.map(lambda a: jnp.bfloat16 if a.dtype == jnp.float32 else a.dtype, x),
    )
    state = jax.tree.map(lambda a, e: jnp.zeros_like(a) + jnp.asarray(e, a.dtype), x, neutral)

    def one(step, state):
        source = count - 1 - step if backward else step
        return join(
            state,
            jax.tree.map(
                lambda a, own: lax.dynamic_index_in_dim(a, source, 0, False).astype(own.dtype),
                gathered,
                x,
            ),
        )

    return lax.fori_loop(0, ahead, one, state)


def combine_spans(earlier, later):
    return (earlier[0] * later[0], later[1] + later[0][..., None] * earlier[1])


def contract_rows(left_mat, right_mat):
    return lax.dot_general(
        left_mat, right_mat, (((0,), (0,)), ((), ())), preferred_element_type=jnp.float32
    )


def contract_cols(left_mat, right_mat):
    return lax.dot_general(
        left_mat, right_mat, (((1,), (1,)), ((), ())), preferred_element_type=jnp.float32
    )


def to_blocks(tensor, head_count):
    rows_here = tensor.shape[0]
    return (
        tensor.astype(jnp.float32)
        .reshape(rows_here // BLOCK, BLOCK, head_count, -1)
        .transpose(2, 0, 1, 3)
    )


def from_blocks(tensor):
    head_count, blocks, _, channels = tensor.shape
    return tensor.transpose(1, 2, 0, 3).reshape(blocks * BLOCK, head_count * channels)


def expert_pass(rows_x, rows_cot, gate_mat, up_mat, down_mat):
    full_x, full_cot = (
        lax.all_gather(rows_x, "tp", axis=1, tiled=True),
        lax.all_gather(rows_cot, "tp", axis=1, tiled=True),
    )
    gate_pre = contract_cols(full_x, gate_mat)
    up_pre = contract_cols(full_x, up_mat)
    sigmoid_gate = jax.nn.sigmoid(gate_pre)
    active = gate_pre * sigmoid_gate
    hidden = (active * up_pre).astype(jnp.bfloat16)
    hidden_cot = contract_cols(full_cot, down_mat)
    up_cot = (hidden_cot * active).astype(jnp.bfloat16)
    gate_cot = (
        hidden_cot * up_pre * sigmoid_gate * (1.0 + gate_pre * (1.0 - sigmoid_gate))
    ).astype(jnp.bfloat16)
    down_g = contract_rows(hidden, full_cot)
    gate_g = contract_rows(gate_cot, full_x)
    up_g = contract_rows(up_cot, full_x)
    dims = (((0,), (1,)), ((), ()))
    first_part = lax.dot_general(gate_mat, gate_cot, dims, preferred_element_type=jnp.float32)
    back_terms = lax.psum_scatter(
        (
            first_part + lax.dot_general(up_mat, up_cot, dims, preferred_element_type=jnp.float32)
        ).astype(jnp.bfloat16),
        "tp",
        scatter_dimension=0,
        tiled=True,
    ).astype(jnp.float32)
    return (gate_g, up_g, down_g, back_terms)


def local(
    layer_in,
    out_cot,
    route_ids,
    route_probs,
    group_prob,
    gate_weight,
    up_weight,
    down_weight,
    out_weight,
    query,
    key_in,
    value,
    decay_logit,
):
    tok_rows = layer_in.shape[0]
    local_cols = layer_in.shape[1]
    experts_all = lax.axis_size("sp")
    capacity = 4 * tok_rows // experts_all
    route_weight = group_prob[:, None] * route_probs / jnp.sum(route_probs, axis=1, keepdims=True)
    chosen = (route_ids[:, :, None] == jnp.arange(experts_all, dtype=jnp.int32)).astype(jnp.int32)
    running = jnp.cumsum(chosen.reshape(2 * tok_rows, experts_all), axis=0).reshape(
        tok_rows, 2, experts_all
    )
    position = jnp.sum((running - 1) * chosen, axis=2)
    slot_ids = route_ids * capacity + position
    matches = (
        slot_ids[None, :, :] == jnp.arange(experts_all * capacity, dtype=jnp.int32)[:, None, None]
    )
    select_x = jnp.any(matches, axis=2).astype(jnp.float32)
    select_cot = jnp.sum(jnp.where(matches, route_weight[None], 0.0), axis=2)
    send_x = jnp.dot(
        select_x.astype(jnp.bfloat16), layer_in, preferred_element_type=jnp.float32
    ).astype(jnp.bfloat16)
    send_cot = jnp.dot(select_cot, out_cot.astype(jnp.float32), precision=highest).astype(
        jnp.bfloat16
    )
    send_x = send_x.reshape(experts_all, capacity, local_cols)
    send_cot = send_cot.reshape(experts_all, capacity, local_cols)
    recv_x, recv_cot = (
        lax.all_to_all(send_x, "sp", split_axis=0, concat_axis=0, tiled=True),
        lax.all_to_all(send_cot, "sp", split_axis=0, concat_axis=0, tiled=True),
    )
    head_dev = query.shape[1] // DK
    scaled_query = to_blocks(query, head_dev) * DK ** (-0.5)
    key_blk = to_blocks(key_in, head_dev)
    value_blk = to_blocks(value, head_dev)
    logit_blk = to_blocks(decay_logit, head_dev)
    cumulative = jnp.cumsum(jax.nn.log_sigmoid(logit_blk) / decay_temp, axis=2)
    span_log = cumulative[:, :, -1:, :]
    growth = jnp.exp(cumulative)
    shrink = jnp.exp(-cumulative)
    to_end = jnp.exp(span_log - cumulative)
    query_decayed = scaled_query * growth
    key_back = key_blk * shrink
    key_to_end = key_blk * to_end
    causal = jnp.tril(jnp.ones((BLOCK, BLOCK), dtype=bool))
    scores = jnp.where(
        causal, jnp.einsum("hncd,hnsd->hncs", query_decayed, key_back, precision=highest), 0.0
    )
    within = jnp.einsum("hncs,hnsv->hncv", scores, value_blk, precision=highest)
    block_decay = jnp.moveaxis(jnp.exp(span_log[:, :, 0, :]), 1, 0)
    block_update = jnp.moveaxis(
        jnp.einsum("hncd,hncv->hndv", key_to_end, value_blk, precision=highest), 1, 0
    )
    identity_pair = (
        jnp.ones((head_dev, DK), jnp.float32),
        jnp.zeros((head_dev, DK, DV), jnp.float32),
    )

    def advance(carry_pair, inputs):
        return (combine_spans(carry_pair, inputs), carry_pair)

    span_total, before_pairs = lax.scan(advance, identity_pair, (block_decay, block_update))
    entry_pair = prefix(span_total, "sp", combine_spans, identity_pair, False)
    entry_state = entry_pair[1]
    decay_before = jnp.moveaxis(before_pairs[0], 0, 1)
    block_state = decay_before[..., None] * entry_state[:, None] + jnp.moveaxis(
        before_pairs[1], 0, 1
    )
    span_end = span_total[0][..., None] * entry_state + span_total[1]
    outputs = within + jnp.einsum("hncd,hndv->hncv", query_decayed, block_state, precision=highest)
    mixer_out = from_blocks(outputs).astype(jnp.bfloat16)
    gate_mat, up_mat, down_mat = (gate_weight[0], up_weight[0], down_weight[0])
    gate_g, up_g, down_g, back_flat = expert_pass(
        recv_x.reshape(-1, local_cols), recv_cot.reshape(-1, local_cols), gate_mat, up_mat, down_mat
    )
    back_terms = back_flat.reshape(local_cols, experts_all, capacity)
    returned = lax.all_to_all(
        back_terms.astype(jnp.bfloat16), "sp", split_axis=1, concat_axis=1, tiled=True
    ).astype(back_terms.dtype)
    returned = returned.reshape(local_cols, experts_all * capacity)
    routed_sum = lax.dot_general(
        select_x,
        returned,
        (((0,), (1,)), ((), ())),
        precision=highest,
        preferred_element_type=jnp.float32,
    )
    mixed_cot = (out_cot.astype(jnp.float32) + routed_sum).astype(jnp.bfloat16)
    full_cot = lax.all_gather(mixed_cot, "tp", axis=1, tiled=True)
    mixer_cot = jnp.dot(full_cot, out_weight, preferred_element_type=jnp.float32)
    proj_grad = lax.psum_scatter(
        contract_rows(full_cot, mixer_out).astype(jnp.bfloat16),
        "sp",
        scatter_dimension=0,
        tiled=True,
    ).astype(jnp.float32)
    cot_blk = to_blocks(mixer_cot, head_dev)
    block_future = jnp.moveaxis(
        jnp.einsum("hncd,hncv->hndv", query_decayed, cot_blk, precision=highest), 1, 0
    )

    def retreat(carry_pair, inputs):
        return (combine_spans(carry_pair, inputs), carry_pair)

    span_back, after_pairs = lax.scan(
        retreat, identity_pair, (block_decay, block_future), reverse=True
    )
    beyond_pair = prefix(span_back, "sp", combine_spans, identity_pair, True)
    future_state = beyond_pair[1]
    decay_after = jnp.moveaxis(after_pairs[0], 0, 1)
    block_future_state = decay_after[..., None] * future_state[:, None] + jnp.moveaxis(
        after_pairs[1], 0, 1
    )
    cot_values = jnp.where(
        causal, jnp.einsum("hncv,hnsv->hncs", cot_blk, value_blk, precision=highest), 0.0
    )
    query_scaled_grad = growth * (
        jnp.einsum("hncv,hndv->hncd", cot_blk, block_state, precision=highest)
        + jnp.einsum("hncs,hnsd->hncd", cot_values, key_back, precision=highest)
    )
    key_part = shrink * jnp.einsum("hncs,hncd->hnsd", cot_values, query_decayed, precision=highest)
    key_grad = key_part + to_end * jnp.einsum(
        "hnsv,hndv->hnsd", value_blk, block_future_state, precision=highest
    )
    value_grad = jnp.einsum("hncs,hncv->hnsv", scores, cot_blk, precision=highest) + jnp.einsum(
        "hnsd,hndv->hnsv", key_to_end, block_future_state, precision=highest
    )
    decay_terms = (scaled_query * query_scaled_grad - key_blk * key_grad).reshape(
        head_dev, tok_rows, DK
    )
    tail_sum = jnp.flip(jnp.cumsum(jnp.flip(decay_terms, 1), axis=1), 1)
    beyond_term = jnp.sum(future_state * span_end, axis=2)
    log_grad = tail_sum + beyond_term[:, None, :]
    logit_flat = logit_blk.reshape(head_dev, tok_rows, DK)
    logit_grad = (
        (log_grad * jax.nn.sigmoid(-logit_flat) / decay_temp)
        .transpose(1, 0, 2)
        .reshape(tok_rows, head_dev * DK)
    )
    query_grad = from_blocks(query_scaled_grad * DK ** (-0.5))
    return (
        gate_g[None],
        up_g[None],
        down_g[None],
        proj_grad,
        query_grad,
        from_blocks(key_grad),
        from_blocks(value_grad),
        logit_grad,
    )


RING = 4


def ring_place(index):
    return index + (index // 2) * (1 - 2 * (index % 2))


def neighbours():
    sp, tp = lax.axis_index("sp"), lax.axis_index("tp")
    chip, core = tp // 2, tp % 2
    place = ring_place(sp)
    sp_at = lambda step: ring_place((place + step) % RING)
    chip_at = lambda step: (chip + step) % RING
    return sp, chip, core, sp_at, chip_at


def remote(source, target, send_sem, recv_sem, device):
    return pltpu.make_async_remote_copy(
        src_ref=source,
        dst_ref=target,
        send_sem=send_sem,
        recv_sem=recv_sem,
        device_id=device,
        device_id_type=pl.DeviceIdType.MESH,
    )


def greet(devices):
    barrier = pltpu.get_barrier_semaphore()
    for device in devices:
        pl.semaphore_signal(
            barrier, inc=1, device_id=device, device_id_type=pl.DeviceIdType.MESH
        )
    pl.semaphore_wait(barrier, len(devices))


def gather_kernel(
    x_ref, cot_ref, small_ref, state_ref,
    x_out, cot_out, small_out, state_out,
    local_sem, first_send, first_recv, second_send, second_recv,
    pair_send, pair_recv, small_send, small_recv, state_send, state_recv,
):
    sp, chip, core, sp_at, chip_at = neighbours()
    tp = 2 * chip + core
    half, width = x_ref.shape[0] // 2, x_ref.shape[1]
    ins, outs = (x_ref, cot_ref), (x_out, cot_out)
    on_sp = lambda step: (sp_at(step), tp)
    on_chip = lambda step: (sp, 2 * chip_at(step) + core)
    pair = (sp, 2 * chip + 1 - core)
    greet([on_sp(1), on_sp(2), on_sp(3), on_chip(1), on_chip(3), pair])

    def cols(chip_no, core_no):
        return pl.ds(pl.multiple_of((2 * chip_no + core_no) * width, width), width)

    def rows(h):
        return pl.ds(h * half, half)

    own = [
        pltpu.make_async_copy(
            ins[a], outs[a].at[sp, :, cols(chip, core)], local_sem.at[a]
        )
        for a in range(2)
    ]
    own_small = [
        pltpu.make_async_copy(small_ref, small_out.at[sp], local_sem.at[2]),
        pltpu.make_async_copy(state_ref, state_out.at[sp], local_sem.at[3]),
    ]
    sends = []
    for step in (1, 3, 2):
        for ref, out, s_sem, r_sem in (
            (small_ref, small_out, small_send, small_recv),
            (state_ref, state_out, state_send, state_recv),
        ):
            copy = remote(ref, out.at[sp], s_sem.at[step - 1], r_sem.at[3 - step], on_sp(step))
            copy.start()
            sends.append(copy)

    def go(copy):
        copy.start()
        sends.append(copy)
        return copy

    def first_region(a, h, step):
        if h == 0:
            return outs[a].at[sp_at(step), rows(h), cols(chip, core)]
        return outs[a].at[sp, rows(h), cols(chip_at(step), core)]

    def second_region(a, h, step, core_no):
        if h == 0:
            return outs[a].at[:, rows(h), cols(chip_at(step), core_no)]
        at = pl.ds(0, 2 * RING * width)
        return outs[a].at[sp_at(step), rows(h), at]

    def first_device(h, step):
        return on_sp(step) if h == 0 else on_chip(step)

    def second_device(h, step):
        return on_chip(step) if h == 0 else on_sp(step)

    for a in range(2):
        for h in range(2):
            for step in (1, 3):
                k = 0 if step == 1 else 1
                go(remote(
                    ins[a].at[rows(h), :], first_region(a, h, 0),
                    first_send.at[a, h, k], first_recv.at[a, h, 3 - step],
                    first_device(h, step),
                ))
    for copy in own + own_small:
        copy.start()

    def arrived(sem, region):
        pltpu.make_async_copy(region, region, sem).wait()

    for a in range(2):
        onward = 1 if a == 0 else 3
        source = 4 - onward
        for h in range(2):
            region = first_region(a, h, source)
            arrived(first_recv.at[a, h, source - 1], region)
            go(remote(
                region, region, first_send.at[a, h, 2], first_recv.at[a, h, 1],
                first_device(h, onward),
            ))
    for copy in own:
        copy.wait()

    def mine(a, h, step):
        if h == 0:
            return [second_region(a, 0, step, core)]
        return [outs[a].at[sp_at(step), rows(1), cols(z, core)] for z in range(RING)]

    for a in range(2):
        onward = 1 if a == 0 else 3
        for h in range(2):
            arrived(first_recv.at[a, h, onward - 1], first_region(a, h, onward))
            arrived(first_recv.at[a, h, 1], first_region(a, h, 2))
            for step in (1, 3):
                k = 0 if step == 1 else 1
                for i, region in enumerate(mine(a, h, 0)):
                    go(remote(
                        region, region, second_send.at[a, h, k, i],
                        second_recv.at[a, h, 3 - step, i], second_device(h, step),
                    ))
            for i, region in enumerate(mine(a, h, 0)):
                go(remote(region, region, pair_send.at[a, h, 0, i], pair_recv.at[a, h, 0, i], pair))

    def relay(a, h, step, onward):
        for i, region in enumerate(mine(a, h, step)):
            arrived(second_recv.at[a, h, step - 1, i], region)
            if onward is not None:
                go(remote(
                    region, region, second_send.at[a, h, 2, i], second_recv.at[a, h, 1, i],
                    second_device(h, onward),
                ))
            go(remote(
                region, region, pair_send.at[a, h, step, i], pair_recv.at[a, h, step, i], pair,
            ))

    for h in range(2):
        relay(0, h, 3, 1)
    for h in range(2):
        relay(1, h, 1, 3)
    for h in range(2):
        relay(0, h, 1, None)
    for h in range(2):
        relay(1, h, 3, None)
    for a in range(2):
        for h in range(2):
            relay(a, h, 2, None)
    for a in range(2):
        for h in range(2):
            for step in range(RING):
                if h == 0:
                    arrived(pair_recv.at[a, h, step, 0], second_region(a, 0, step, 1 - core))
                else:
                    for z in range(RING):
                        arrived(
                            pair_recv.at[a, h, step, z],
                            outs[a].at[sp_at(step), rows(1), cols(z, 1 - core)],
                        )
    for copy in own_small:
        copy.wait()
    for step in (1, 2, 3):
        arrived(small_recv.at[step - 1], small_out.at[sp_at(step)])
        arrived(state_recv.at[step - 1], state_out.at[sp_at(step)])
    for copy in sends:
        copy.wait_send()


def gather_rows(x, cot, small, state):
    tok_rows, width = x.shape
    full = (RING, tok_rows, 2 * RING * width)
    vmem = pl.BlockSpec(memory_space=pltpu.VMEM)
    dma = pltpu.SemaphoreType.DMA
    return pl.pallas_call(
        gather_kernel,
        out_shape=[
            jax.ShapeDtypeStruct(full, x.dtype),
            jax.ShapeDtypeStruct(full, cot.dtype),
            jax.ShapeDtypeStruct((RING,) + small.shape, small.dtype),
            jax.ShapeDtypeStruct((RING,) + state.shape, state.dtype),
        ],
        in_specs=[vmem] * 4,
        out_specs=[pl.BlockSpec(memory_space=pltpu.HBM)] * 2 + [vmem] * 2,
        scratch_shapes=[
            dma((4,)),
            dma((2, 2, 3)), dma((2, 2, 3)),
            dma((2, 2, 3, RING)), dma((2, 2, 3, RING)),
            dma((2, 2, 4, RING)), dma((2, 2, 4, RING)),
            dma((3,)), dma((3,)), dma((3,)), dma((3,)),
        ],
        compiler_params=pltpu.CompilerParams(collective_id=0, has_side_effects=True),
        name="gather_rows",
    )(x, cot, small, state)


def small_kernel(x_ref, out_ref, local_sem, send_sem, recv_sem):
    sp, chip, core, sp_at, chip_at = neighbours()
    tp = 2 * chip + core
    greet([(sp_at(step), tp) for step in (1, 2, 3)])
    sends = []
    for step in (2, 1, 3):
        copy = remote(
            x_ref, out_ref.at[sp], send_sem.at[step - 1], recv_sem.at[3 - step],
            (sp_at(step), tp),
        )
        copy.start()
        sends.append(copy)
    own = pltpu.make_async_copy(x_ref, out_ref.at[sp], local_sem)
    own.start()
    own.wait()
    for step in (1, 2, 3):
        region = out_ref.at[sp_at(step)]
        pltpu.make_async_copy(region, region, recv_sem.at[step - 1]).wait()
    for copy in sends:
        copy.wait_send()


def gather_small(x):
    vmem = pl.BlockSpec(memory_space=pltpu.VMEM)
    dma = pltpu.SemaphoreType.DMA
    return pl.pallas_call(
        small_kernel,
        out_shape=jax.ShapeDtypeStruct((RING,) + x.shape, x.dtype),
        in_specs=[vmem],
        out_specs=vmem,
        scratch_shapes=[dma, dma((3,)), dma((3,))],
        compiler_params=pltpu.CompilerParams(collective_id=1, has_side_effects=True),
        name="gather_small",
    )(x)


def ring_local(
    layer_in, out_cot, route_ids, route_probs, group_prob, gate_weight, up_weight,
    down_weight, out_weight, query, key_in, value, decay_logit,
):
    tok_rows, local_cols = layer_in.shape
    experts_all = lax.axis_size("sp")
    here = lax.axis_index("sp")
    route_weight = group_prob[:, None] * route_probs / jnp.sum(route_probs, axis=1, keepdims=True)
    table = jnp.sum(
        jnp.where(
            route_ids[None] == jnp.arange(experts_all, dtype=jnp.int32)[:, None, None],
            route_weight[None],
            0.0,
        ),
        axis=2,
    )
    head_dev = query.shape[1] // DK
    scaled_query = to_blocks(query, head_dev) * DK ** (-0.5)
    key_blk = to_blocks(key_in, head_dev)
    value_blk = to_blocks(value, head_dev)
    logit_blk = to_blocks(decay_logit, head_dev)
    blocks = key_blk.shape[1]
    causal = jnp.tril(jnp.ones((BLOCK, BLOCK), dtype=bool))
    cumulative = jnp.einsum(
        "cs,hnsd->hncd",
        causal.astype(jnp.float32),
        jax.nn.log_sigmoid(logit_blk) / decay_temp,
        precision=highest,
    )
    span_log = cumulative[:, :, -1:, :]
    growth = jnp.exp(cumulative)
    shrink = jnp.exp(-cumulative)
    to_end = jnp.exp(span_log - cumulative)
    query_decayed = scaled_query * growth
    key_back = key_blk * shrink
    key_to_end = key_blk * to_end
    block_decay = jnp.exp(span_log[:, :, 0, :])
    block_update = jnp.einsum("hncd,hncv->hndv", key_to_end, value_blk, precision=highest)
    befores, state = [], jnp.zeros((head_dev, DK, DV), jnp.float32)
    for n in range(blocks):
        befores.append(state)
        state = state * block_decay[:, n, :, None] + block_update[:, n]
    span_state = state
    total_log = jnp.sum(span_log[:, :, 0, :], axis=1)
    span_decay = jnp.exp(total_log)
    lanes = -(-max(tok_rows, head_dev * DK) // 128) * 128
    small = jnp.zeros((8, lanes), jnp.float32)
    small = small.at[:experts_all, :tok_rows].set(table)
    small = small.at[experts_all, : head_dev * DK].set(span_decay.reshape(-1))
    full_x, full_cot, smalls, states = gather_rows(
        layer_in, out_cot, small, span_state.astype(jnp.bfloat16).reshape(head_dev * DK, DV)
    )
    all_rows = RING * tok_rows
    full_x = full_x.reshape(all_rows, -1)
    full_cot = full_cot.reshape(all_rows, -1)
    weights = lax.dynamic_index_in_dim(smalls, here, 1, False)[:, :tok_rows].reshape(all_rows, 1)
    decays = smalls[:, experts_all, : head_dev * DK].reshape(RING, head_dev, DK, 1)
    states = states.astype(jnp.float32).reshape(RING, head_dev, DK, DV)
    entry_state = jnp.zeros((head_dev, DK, DV), jnp.float32)
    for s in range(RING - 1):
        entry_state = jnp.where(s < here, entry_state * decays[s] + states[s], entry_state)

    gate_mat, up_mat, down_mat = (gate_weight[0], up_weight[0], down_weight[0])
    gate_pre = contract_cols(full_x, gate_mat)
    up_pre = contract_cols(full_x, up_mat)
    sigmoid_gate = jax.nn.sigmoid(gate_pre)
    active = gate_pre * sigmoid_gate
    hidden = (active * up_pre * weights).astype(jnp.bfloat16)
    hidden_cot = contract_cols(full_cot, down_mat) * weights
    up_cot = (hidden_cot * active).astype(jnp.bfloat16)
    gate_cot = (
        hidden_cot * up_pre * sigmoid_gate * (1.0 + gate_pre * (1.0 - sigmoid_gate))
    ).astype(jnp.bfloat16)
    back = (
        jnp.dot(gate_cot, gate_mat, preferred_element_type=jnp.float32)
        + jnp.dot(up_cot, up_mat, preferred_element_type=jnp.float32)
    ).astype(jnp.bfloat16)
    back_terms = lax.psum_scatter(back, "tp", scatter_dimension=1, tiled=True)
    returned = lax.all_to_all(
        back_terms.reshape(RING, tok_rows, local_cols), "sp", split_axis=0, concat_axis=0, tiled=True
    )
    down_g = contract_rows(hidden, full_cot)
    gate_g = contract_rows(gate_cot, full_x)
    up_g = contract_rows(up_cot, full_x)
    mixed_cot = (
        out_cot.astype(jnp.float32) + jnp.sum(returned.astype(jnp.float32), axis=0)
    ).astype(jnp.bfloat16)
    full_mixed = lax.all_gather(mixed_cot, "tp", axis=1, tiled=True)

    entering = []
    for n in range(blocks):
        entering.append(entry_state if n == 0 else entering[-1] * block_decay[:, n - 1, :, None] + block_update[:, n - 1])
    span_end = span_decay[..., None] * entry_state + span_state
    block_state = jnp.stack(entering, axis=1)
    scores = jnp.where(
        causal, jnp.einsum("hncd,hnsd->hncs", query_decayed, key_back, precision=highest), 0.0
    )
    outputs = jnp.einsum(
        "hncs,hnsv->hncv", scores, value_blk, precision=highest
    ) + jnp.einsum("hncd,hndv->hncv", query_decayed, block_state, precision=highest)
    mixer_out = from_blocks(outputs).astype(jnp.bfloat16)

    mixer_cot = jnp.dot(full_mixed, out_weight, preferred_element_type=jnp.float32)
    proj_grad = lax.psum_scatter(
        contract_rows(full_mixed, mixer_out).astype(jnp.bfloat16),
        "sp",
        scatter_dimension=0,
        tiled=True,
    ).astype(jnp.float32)
    cot_blk = to_blocks(mixer_cot, head_dev)
    block_future = jnp.einsum("hncd,hncv->hndv", query_decayed, cot_blk, precision=highest)
    span_future = jnp.zeros((head_dev, DK, DV), jnp.float32)
    for n in range(blocks - 1, -1, -1):
        span_future = span_future * block_decay[:, n, :, None] + block_future[:, n]
    futures = gather_small(span_future.astype(jnp.bfloat16).reshape(head_dev * DK, DV))
    futures = futures.astype(jnp.float32).reshape(RING, head_dev, DK, DV)
    future_state = jnp.zeros((head_dev, DK, DV), jnp.float32)
    for s in range(RING - 1, 0, -1):
        future_state = jnp.where(s > here, future_state * decays[s] + futures[s], future_state)
    leaving = [future_state]
    for n in range(blocks - 1, 0, -1):
        leaving.append(leaving[-1] * block_decay[:, n, :, None] + block_future[:, n])
    block_future_state = jnp.stack(leaving[::-1], axis=1)
    cot_values = jnp.where(
        causal, jnp.einsum("hncv,hnsv->hncs", cot_blk, value_blk, precision=highest), 0.0
    )
    query_scaled_grad = growth * (
        jnp.einsum("hncv,hndv->hncd", cot_blk, block_state, precision=highest)
        + jnp.einsum("hncs,hnsd->hncd", cot_values, key_back, precision=highest)
    )
    key_part = shrink * jnp.einsum("hncs,hncd->hnsd", cot_values, query_decayed, precision=highest)
    key_grad = key_part + to_end * jnp.einsum(
        "hnsv,hndv->hnsd", value_blk, block_future_state, precision=highest
    )
    value_grad = jnp.einsum("hncs,hncv->hnsv", scores, cot_blk, precision=highest) + jnp.einsum(
        "hnsd,hndv->hnsv", key_to_end, block_future_state, precision=highest
    )
    decay_terms = scaled_query * query_scaled_grad - key_blk * key_grad
    within_tail = jnp.einsum(
        "cs,hncd->hnsd", causal.astype(jnp.float32), decay_terms, precision=highest
    )
    beyond_term = jnp.sum(future_state * span_end, axis=2)
    tails, run = [], beyond_term
    for n in range(blocks - 1, -1, -1):
        tails.append(run)
        run = run + within_tail[:, n, 0]
    log_grad = within_tail + jnp.stack(tails[::-1], axis=1)[:, :, None, :]
    logit_grad = from_blocks(log_grad * jax.nn.sigmoid(-logit_blk) / decay_temp)
    return (
        gate_g[None], up_g[None], down_g[None], proj_grad,
        from_blocks(query_scaled_grad * DK ** (-0.5)),
        from_blocks(key_grad), from_blocks(value_grad), logit_grad,
    )


def solution(mesh):
    in_specs = (
        P("sp", "tp"),
        P("sp", "tp"),
        P("sp", None),
        P("sp", None),
        P("sp"),
        P("sp", "tp", None),
        P("sp", "tp", None),
        P("sp", "tp", None),
        P(None, "tp"),
        P("sp", "tp"),
        P("sp", "tp"),
        P("sp", "tp"),
        P("sp", "tp"),
    )
    out_specs = (
        P("sp", "tp", None),
        P("sp", "tp", None),
        P("sp", "tp", None),
        P("sp", "tp"),
        P("sp", "tp"),
        P("sp", "tp"),
        P("sp", "tp"),
        P("sp", "tp"),
    )
    rows = 4 // mesh.shape["sp"]
    body = ring_local if rows * 4 == 4 and mesh.shape["tp"] == 8 else local
    return jax.shard_map(body, mesh=mesh, in_specs=in_specs, out_specs=out_specs, check_vma=False)
```

profile of v0, /device:TPU:0, one launch (start us, length us, event | category | flops | bytes accessed | tf_op | source)
XLA Modules:
  0.0 256.0 jit_solution(3788196213773021022)
XLA Ops:
  7.3 1.7 fusion.55
  13.6 66.1 %gather_rows.1 = (bf16[4,320,2048]{2,1,0:T(8,128)(2,1)}, bf16[4,320,2048]{2,1,0:T(8,128)(2,1)}, f32[4,8,384]{2,1,0:T(8,128)}, bf16[4,128,128]{2,1,0:T(8,128)(2,1)}) custom-call(bf16[320,256]{1,0:T(8,128)(2,1)} %x_ref.1, bf16[320,256]{1,0:T(8,128)(2,1)} %cot_ref.1, f32[8,384]{1,0:T(8,128)} %copy-done.33, bf16[128,128]{1,0:T(8,128)(2,1)} %fusion.77.state_ref), custom_call_target="tpu_custom_call" | custom-call | tf_op jit(solution)/shard_map/gather_rows/pallas_call | solution.py:463
  79.8 5.3 %fusion.6 = f32[1280,256]{1,0:T(8,128)} fusion(bf16[1280,2048]{1,0:T(8,128)(2,1)} %bitcast.321, bf16[1,256,2048]{2,1,0:T(8,128)(2,1)S(1)} %copy-done), kind=kOutput, calls=%fused_computation.22 | convolution fusion | flops 1342177280 | bytes 7602176 | tf_op jit(solution)/shard_map/dot_general | solution.py:54
  85.1 2.7 %fusion.9 = f32[1280,256]{1,0:T(8,128)} fusion(bf16[1280,2048]{1,0:T(8,128)(2,1)S(1)} %bitcast.323, bf16[1,256,2048]{2,1,0:T(8,128)(2,1)S(1)} %copy-done.13), kind=kOutput, calls=%fused_computation.25 | convolution fusion | flops 1342177280 | bytes 7602176 | tf_op jit(solution)/shard_map/dot_general | solution.py:54
  88.7 5.5 %multiply_convert_fusion.1 = (bf16[1280,256]{1,0:T(8,128)(2,1)S(1)}, bf16[1280,256]{1,0:T(8,128)(2,1)S(1)}) fusion(f32[1280,256]{1,0:T(8,128)} %fusion.6, f32[1280,256]{1,0:T(8,128)} %fusion.9, f32[1280]{0:T(1024)S(1)} %mul.479, bf16[1280,2048]{1,0:T(8,128)(2,1)} %bitcast.352, bf16[1,256,2048]{2,1,0:T(8,128)(2,1)} %param.24), kind=kOutput, calls=%fused_computation.8 | convolution fusion | flops 1346764800 | bytes 10228736 | tf_op jit(solution)/shard_map/dot_general | solution.py:54
  94.2 1.5 fusion.4
  95.8 3.9 %add_convert_fusion = bf16[1280,2048]{1,0:T(8,128)(2,1)} fusion(f32[1280,2048]{1,0:T(8,128)S(1)} %fusion.4, bf16[1280,256]{1,0:T(8,128)(2,1)S(1)} %get-tuple-element.55, bf16[1,256,2048]{2,1,0:T(8,128)(2,1)S(1)} %copy-done.14), kind=kOutput, calls=%fused_computation | convolution fusion | flops 1347420160 | bytes 17432576 | tf_op jit(solution)/shard_map/dot_general | solution.py:596
  99.7 1.8 fusion.86
  101.8 1.6 convert_multiply_fusion
  104.1 55.5 %reduce-scatter.3.cloned.1.call-done = bf16[1280,256]{1,0:T(8,128)(2,1)} async-done(((bf16[1280,2048]{1,0:T(8,128)(2,1)}), bf16[1280,256]{1,0:T(8,128)(2,1)}) %reduce-scatter.3.cloned.1.call-update) | async-done | bytes 655376 | tf_op jit(solution)/shard_map/reduce_scatter | solution.py:598
  159.6 4.3 %all-to-all-start = ((bf16[4,320,256]{2,1,0:T(8,128)(2,1)}), bf16[4,320,256]{2,1,0:T(8,128)(2,1)}, u32[]{:S(2)}, u32[]{:S(2)}) async-start(bf16[4,320,256]{2,1,0:T(8,128)(2,1)} %bitcast.330), calls=%async_computation.1 | async-start | bytes 1310720 | tf_op jit(solution)/shard_map/all_to_all | solution.py:599
  166.7 1.3 mul_broadcast_in_dim.36
  168.0 1.9 div.29
  169.9 1.6 constant_dynamic-update-slice_fusion.2
  171.5 1.7 constant_dynamic-update-slice_fusion.1
  174.3 1.6 add_convert_fusion.1
  178.7 5.9 %convolution_bitcast_fusion.2 = f32[1,256,2048]{2,1,0:T(8,128)} fusion(bf16[1280,256]{1,0:T(8,128)(2,1)S(1)} %get-tuple-element.56, bf16[1280,2048]{1,0:T(8,128)(2,1)} %bitcast.322), kind=kOutput, calls=%fused_computation.4 | convolution fusion | flops 1342177280 | bytes 7995392 | tf_op jit(solution)/shard_map/dot_general | solution.py:48
  184.7 2.9 %convolution_bitcast_fusion.1 = f32[1,256,2048]{2,1,0:T(8,128)} fusion(bf16[1280,256]{1,0:T(8,128)(2,1)S(1)} %get-tuple-element.55, bf16[1280,2048]{1,0:T(8,128)(2,1)S(1)} %bitcast.326), kind=kOutput, calls=%fused_computation.3 | convolution fusion | flops 1342177280 | bytes 7995392 | tf_op jit(solution)/shard_map/dot_general | solution.py:48
  187.6 3.0 %convolution_bitcast_fusion = f32[1,256,2048]{2,1,0:T(8,128)} fusion(bf16[1280,2048]{1,0:T(8,128)(2,1)S(1)} %bitcast.355, f32[1280,256]{1,0:T(8,128)S(1)} %copy-done.67, f32[1280]{0:T(1024)S(1)} %copy-done.36, f32[1280,256]{1,0:T(8,128)S(1)} %copy-done.66), kind=kOutput, calls=%fused_computation.2 | convolution fusion | flops 1344471040 | bytes 9966592 | tf_op jit(solution)/shard_map/dot_general | solution.py:48
  190.6 10.0 %all-gather.2.cloned.1.call-done = bf16[320,2048]{1,0:T(8,128)(2,1)} async-done(((bf16[320,256]{1,0:T(8,128)(2,1)}), bf16[320,2048]{1,0:T(8,128)(2,1)}) %all-gather.2.cloned.1.call-update) | async-done | bytes 1310736 | tf_op jit(solution)/shard_map/all_gather | solution.py:608
  200.6 2.1 fusion.104
  204.6 6.3 %gather_small.1 = bf16[4,128,128]{2,1,0:T(8,128)(2,1)} custom-call(bf16[128,128]{1,0:T(8,128)(2,1)} %fusion.72.x_ref), custom_call_target="tpu_custom_call" | custom-call | tf_op jit(solution)/shard_map/gather_small/pallas_call | solution.py:510
  212.7 1.6 constant_dynamic-update-slice_fusion.7
  215.0 2.2 fusion.31
  218.7 1.8 convolution_convert_fusion
  221.0 1.3 convolution_add_fusion.1
  225.2 1.9 reshape.626
  227.1 1.9 copy.93
  229.0 1.9 reshape.627
  231.5 1.4 fusion.1
  236.6 11.0 %reduce-scatter.5.cloned.1.call-done = bf16[512,256]{1,0:T(8,128)(2,1)} async-done(((bf16[2048,256]{1,0:T(8,128)(2,1)}), bf16[512,256]{1,0:T(8,128)(2,1)}) %reduce-scatter.5.cloned.1.call-update) | async-done | bytes 262160 | tf_op jit(solution)/shard_map/reduce_scatter | solution.py:624
  247.6 1.8 convert_element_type.75
  (228 shorter events, 26.2 us)
Async XLA Ops:
  7.2 72.6 %copy-start = (bf16[1,256,2048]{2,1,0:T(8,128)(2,1)S(1)}, bf16[1,256,2048]{2,1,0:T(8,128)(2,1)}, u32[]{:S(2)}) copy-start(bf16[1,256,2048]{2,1,0:T(8,128)(2,1)} %param.22) | copy-start | bytes 3145732
  7.2 152.4 %reduce-scatter.3.cloned.1.call-start = ((), (), s32[]{:S(2)}) async-start(), calls=%async_computation.3 | async-start | bytes 5898240 | tf_op jit(solution)/shard_map/reduce_scatter | solution.py:598
  11.5 73.5 %copy-start.20 = (f32[2,1,64,128]{3,2,1,0:T(8,128)}, f32[2,1,64,128]{3,2,1,0:T(8,128)S(1)}, u32[]{:S(2)}) copy-start(f32[2,1,64,128]{3,2,1,0:T(8,128)S(1)} %get-tuple-element.68) | copy-start | bytes 196612
  11.5 73.5 %copy-start.22 = (f32[2,1,64,128]{3,2,1,0:T(8,128)}, f32[2,1,64,128]{3,2,1,0:T(8,128)S(1)}, u32[]{:S(2)}) copy-start(f32[2,1,64,128]{3,2,1,0:T(8,128)S(1)} %get-tuple-element.69) | copy-start | bytes 196612
  11.6 73.5 %copy-start.24 = (f32[2,1,64,128]{3,2,1,0:T(8,128)}, f32[2,1,64,128]{3,2,1,0:T(8,128)S(1)}, u32[]{:S(2)}) copy-start(f32[2,1,64,128]{3,2,1,0:T(8,128)S(1)} %get-tuple-element.70) | copy-start | bytes 196612
  11.6 73.5 %copy-start.26 = (f32[2,1,64,128]{3,2,1,0:T(8,128)}, f32[2,1,64,128]{3,2,1,0:T(8,128)S(1)}, u32[]{:S(2)}) copy-start(f32[2,1,64,128]{3,2,1,0:T(8,128)S(1)} %get-tuple-element.71) | copy-start | bytes 196612
  11.6 73.5 %copy-start.28 = (f32[2,1,64,128]{3,2,1,0:T(8,128)}, f32[2,1,64,128]{3,2,1,0:T(8,128)S(1)}, u32[]{:S(2)}) copy-start(f32[2,1,64,128]{3,2,1,0:T(8,128)S(1)} %get-tuple-element.72) | copy-start | bytes 196612
  12.3 72.8 %copy-start.49 = (f32[128]{0:T(128)}, f32[128]{0:T(128)S(1)}, u32[]{:S(2)}) copy-start(f32[128]{0:T(128)S(1)} %mul.476) | copy-start | bytes 1540
  12.4 72.7 %copy-start.37 = (f32[128]{0:T(128)}, f32[128]{0:T(128)S(1)}, u32[]{:S(2)}) copy-start(f32[128]{0:T(128)S(1)} %mul.473) | copy-start | bytes 1540
  12.5 72.6 %copy-start.39 = (f32[128]{0:T(128)}, f32[128]{0:T(128)S(1)}, u32[]{:S(2)}) copy-start(f32[128]{0:T(128)S(1)} %mul.470) | copy-start | bytes 1540
  12.5 72.6 %copy-start.41 = (f32[128]{0:T(128)}, f32[128]{0:T(128)S(1)}, u32[]{:S(2)}) copy-start(f32[128]{0:T(128)S(1)} %mul.467) | copy-start | bytes 1540
  12.6 72.5 %copy-start.62 = (f32[128]{0:T(128)}, f32[128]{0:T(128)S(1)}, u32[]{:S(2)}) copy-start(f32[128]{0:T(128)S(1)} %mul.464) | copy-start | bytes 1540
  12.6 72.5 %copy-start.52 = (f32[128]{0:T(128)}, f32[128]{0:T(128)S(1)}, u32[]{:S(2)}) copy-start(f32[128]{0:T(128)S(1)} %broadcast_multiply_fusion.1) | copy-start | bytes 1540
  79.8 5.4 %copy-start.1 = (bf16[4,320,2048]{2,1,0:T(8,128)(2,1)S(1)}, bf16[4,320,2048]{2,1,0:T(8,128)(2,1)}, u32[]{:S(2)}) copy-start(bf16[4,320,2048]{2,1,0:T(8,128)(2,1)} %get-tuple-element.38) | copy-start | bytes 15728644
  79.8 5.4 %copy-start.13 = (bf16[1,256,2048]{2,1,0:T(8,128)(2,1)S(1)}, bf16[1,256,2048]{2,1,0:T(8,128)(2,1)}, u32[]{:S(2)}) copy-start(bf16[1,256,2048]{2,1,0:T(8,128)(2,1)} %param.23) | copy-start | bytes 3145732
  88.7 5.5 %copy-start.35 = (f32[1280]{0:T(1024)}, f32[1280]{0:T(1024)S(1)}, u32[]{:S(2)}) copy-start(f32[1280]{0:T(1024)S(1)} %mul.479) | copy-start | bytes 15364
  99.7 64.4 %copy-start.60 = (f32[2,64]{1,0:T(2,128)S(1)}, f32[2,64]{1,0:T(2,128)}, u32[]{:S(2)}) copy-start(f32[2,64]{1,0:T(2,128)} %copy-done.59) | copy-start | bytes 1540
  101.6 63.1 %copy-start.44 = (f32[2,64]{1,0:T(2,128)}, f32[2,64]{1,0:T(2,128)S(1)}, u32[]{:S(2)}) copy-start(f32[2,64]{1,0:T(2,128)S(1)} %mul.496) | copy-start | bytes 1540
  101.7 63.1 %copy-start.46 = (f32[2,64]{1,0:T(2,128)}, f32[2,64]{1,0:T(2,128)S(1)}, u32[]{:S(2)}) copy-start(f32[2,64]{1,0:T(2,128)S(1)} %mul.499) | copy-start | bytes 1540
  159.6 13.5 %all-to-all-start = ((bf16[4,320,256]{2,1,0:T(8,128)(2,1)}), bf16[4,320,256]{2,1,0:T(8,128)(2,1)}, u32[]{:S(2)}, u32[]{:S(2)}) async-start(bf16[4,320,256]{2,1,0:T(8,128)(2,1)} %bitcast.330), calls=%async_computation.1 | async-start | bytes 1310720 | tf_op jit(solution)/shard_map/all_to_all | solution.py:599
  164.0 36.6 %all-gather.2.cloned.1.call-start = ((), (), s32[]{:S(2)}) async-start(), calls=%async_computation.4 | async-start | bytes 1474560 | tf_op jit(solution)/shard_map/all_gather | solution.py:608
  168.0 8.0 %copy-start.50 = (f32[128]{0:T(128)S(1)}, f32[128]{0:T(128)}, u32[]{:S(2)}) copy-start(f32[128]{0:T(128)} %copy-done.49) | copy-start | bytes 1540
  176.0 71.7 %reduce-scatter.5.cloned.1.call-start = ((), (), s32[]{:S(2)}) async-start(), calls=%async_computation.5 | async-start | bytes 1310720 | tf_op jit(solution)/shard_map/reduce_scatter | solution.py:624
  176.6 8.1 %slice-start = ((s8[5242880]{0:T(1024)(128)(4,1)}), s8[4194304]{0:T(1024)(128)(4,1)S(1)}, s32[]{:S(2)}) async-start(s8[5242880]{0:T(1024)(128)(4,1)} %bitcast.324), calls=%async_computation.6 | async-start | bytes 8388608
  176.6 11.0 %slice-start.2 = ((s8[5242880]{0:T(1024)(128)(4,1)}), s8[4194304]{0:T(1024)(128)(4,1)S(1)}, s32[]{:S(2)}) async-start(s8[5242880]{0:T(1024)(128)(4,1)} %bitcast.353), calls=%async_computation.8 | async-start | bytes 8388608
  178.7 6.0 %slice-start.1 = ((s8[5242880]{0:T(1024)(128)(4,1)}), s8[1048576]{0:T(1024)(128)(4,1)S(1)}, s32[]{:S(2)}) async-start(s8[5242880]{0:T(1024)(128)(4,1)} %bitcast.324), calls=%async_computation.7 | async-start | bytes 2097152
  178.7 8.9 %slice-start.3 = ((s8[5242880]{0:T(1024)(128)(4,1)}), s8[1048576]{0:T(1024)(128)(4,1)S(1)}, s32[]{:S(2)}) async-start(s8[5242880]{0:T(1024)(128)(4,1)} %bitcast.353), calls=%async_computation.9 | async-start | bytes 2097152
  203.7 8.0 %copy-start.45 = (f32[2,64]{1,0:T(2,128)S(1)}, f32[2,64]{1,0:T(2,128)}, u32[]{:S(2)}) copy-start(f32[2,64]{1,0:T(2,128)} %copy-done.44) | copy-start | bytes 1540
  203.7 8.0 %copy-start.47 = (f32[2,64]{1,0:T(2,128)S(1)}, f32[2,64]{1,0:T(2,128)}, u32[]{:S(2)}) copy-start(f32[2,64]{1,0:T(2,128)} %copy-done.46) | copy-start | bytes 1540
  203.7 9.0 %copy-start.3 = (f32[2,5,64,128]{3,2,1,0:T(8,128)S(1)}, f32[2,5,64,128]{3,2,1,0:T(8,128)}, u32[]{:S(2)}) copy-start(f32[2,5,64,128]{3,2,1,0:T(8,128)} %copy-done.2) | copy-start | bytes 983044
  211.7 5.5 %copy-start.12 = (f32[2,5,64,128]{3,2,1,0:T(8,128)S(1)}, f32[2,5,64,128]{3,2,1,0:T(8,128)}, u32[]{:S(2)}) copy-start(f32[2,5,64,128]{3,2,1,0:T(8,128)} %fusion.61) | copy-start | bytes 983044
  223.5 7.4 %copy-start.5 = (f32[2,5,64,64]{3,2,1,0:T(8,128)S(1)}, f32[2,5,64,64]{3,2,1,0:T(8,128)}, u32[]{:S(2)}) copy-start(f32[2,5,64,64]{3,2,1,0:T(8,128)} %copy-done.4) | copy-start | bytes 491524
  (44 other events, 93.8 us)
Sparse Core Ops, SparseCore 0:
  99.8 59.8 reduce-scatter.2
  176.1 24.4 all-gather.1
  220.6 26.9 reduce-scatter.4
where the time goes:
time: 257 us; the launch traced here: 256 us
  waiting for transfers between devices  76.6 us (30%)
  Pallas kernels  72.4 us (28%)
  matrix products  46.1 us (18%)
  other arithmetic  21 us (8%)
  local copies, waits for them, and re-layouts  20.6 us (8%)
  between operations  14.9 us (6%)
  starting transfers between devices  4.46 us (2%)
    pallas_call x1, Pallas kernels, gather_rows(): pl.pallas_call(gather_kernel, out_shape=[jax.ShapeDtypeStruct(full, x.dty...  66.1 us
    reduce_scatter x1, waiting for transfers between devices, ring_local(): back_terms = lax.psum_scatter(back, 'tp', scatter_dimension=1, tiled=True)  55.5 us
    dot_general x4, matrix products, contract_rows(): lax.dot_general(left_mat, right_mat, (((0,), (0,)), ((), ())), preferred_...  13.6 us
    dot_general x3, matrix products, contract_cols(): lax.dot_general(left_mat, right_mat, (((1,), (1,)), ((), ())), preferred_...  13.4 us
    reduce_scatter x1, waiting for transfers between devices, ring_local(): lax.psum_scatter(contract_rows(full_mixed, mixer_out).astype(jnp.bfloat16...  11 us
    all_gather x1, waiting for transfers between devices, ring_local(): full_mixed = lax.all_gather(mixed_cot, 'tp', axis=1, tiled=True)  9.99 us
    unnamed x8, other arithmetic  6.51 us
    pallas_call x1, Pallas kernels, gather_small(): pl.pallas_call(small_kernel, out_shape=jax.ShapeDtypeStruct((RING,) + x.s...  6.28 us
  transfers between devices with their start and end apart: 4, of which 3 were waited for; matrix products, arithmetic and copies ran while one was open for 17% of the time, Pallas kernels for 0%

commit v1 on v0

v1 whole, which is shorter than its diff:
```python
import functools
import jax
import jax.numpy as jnp
from jax import lax
from jax.experimental import pallas as pl
from jax.experimental.pallas import tpu as pltpu
from jax.sharding import PartitionSpec as P

DK = 64
DV = 128
BLOCK = 64


decay_temp = 16.0
highest = lax.Precision.HIGH


def prefix(x, axis, join, neutral, backward):
    count = lax.axis_size(axis)
    place = lax.axis_index(axis)
    ahead = count - 1 - place if backward else place
    gathered = jax.tree.map(
        lambda a, kind: lax.all_gather(a.astype(kind), axis),
        x,
        jax.tree.map(lambda a: jnp.bfloat16 if a.dtype == jnp.float32 else a.dtype, x),
    )
    state = jax.tree.map(lambda a, e: jnp.zeros_like(a) + jnp.asarray(e, a.dtype), x, neutral)

    def one(step, state):
        source = count - 1 - step if backward else step
        return join(
            state,
            jax.tree.map(
                lambda a, own: lax.dynamic_index_in_dim(a, source, 0, False).astype(own.dtype),
                gathered,
                x,
            ),
        )

    return lax.fori_loop(0, ahead, one, state)


def combine_spans(earlier, later):
    return (earlier[0] * later[0], later[1] + later[0][..., None] * earlier[1])


def contract_rows(left_mat, right_mat):
    return lax.dot_general(
        left_mat, right_mat, (((0,), (0,)), ((), ())), preferred_element_type=jnp.float32
    )


def contract_cols(left_mat, right_mat):
    return lax.dot_general(
        left_mat, right_mat, (((1,), (1,)), ((), ())), preferred_element_type=jnp.float32
    )


def to_blocks(tensor, head_count):
    rows_here = tensor.shape[0]
    return (
        tensor.astype(jnp.float32)
        .reshape(rows_here // BLOCK, BLOCK, head_count, -1)
        .transpose(2, 0, 1, 3)
    )


def from_blocks(tensor):
    head_count, blocks, _, channels = tensor.shape
    return tensor.transpose(1, 2, 0, 3).reshape(blocks * BLOCK, head_count * channels)


def expert_pass(rows_x, rows_cot, gate_mat, up_mat, down_mat):
    full_x, full_cot = (
        lax.all_gather(rows_x, "tp", axis=1, tiled=True),
        lax.all_gather(rows_cot, "tp", axis=1, tiled=True),
    )
    gate_pre = contract_cols(full_x, gate_mat)
    up_pre = contract_cols(full_x, up_mat)
    sigmoid_gate = jax.nn.sigmoid(gate_pre)
    active = gate_pre * sigmoid_gate
    hidden = (active * up_pre).astype(jnp.bfloat16)
    hidden_cot = contract_cols(full_cot, down_mat)
    up_cot = (hidden_cot * active).astype(jnp.bfloat16)
    gate_cot = (
        hidden_cot * up_pre * sigmoid_gate * (1.0 + gate_pre * (1.0 - sigmoid_gate))
    ).astype(jnp.bfloat16)
    down_g = contract_rows(hidden, full_cot)
    gate_g = contract_rows(gate_cot, full_x)
    up_g = contract_rows(up_cot, full_x)
    dims = (((0,), (1,)), ((), ()))
    first_part = lax.dot_general(gate_mat, gate_cot, dims, preferred_element_type=jnp.float32)
    back_terms = lax.psum_scatter(
        (
            first_part + lax.dot_general(up_mat, up_cot, dims, preferred_element_type=jnp.float32)
        ).astype(jnp.bfloat16),
        "tp",
        scatter_dimension=0,
        tiled=True,
    ).astype(jnp.float32)
    return (gate_g, up_g, down_g, back_terms)


def local(
    layer_in,
    out_cot,
    route_ids,
    route_probs,
    group_prob,
    gate_weight,
    up_weight,
    down_weight,
    out_weight,
    query,
    key_in,
    value,
    decay_logit,
):
    tok_rows = layer_in.shape[0]
    local_cols = layer_in.shape[1]
    experts_all = lax.axis_size("sp")
    capacity = 4 * tok_rows // experts_all
    route_weight = group_prob[:, None] * route_probs / jnp.sum(route_probs, axis=1, keepdims=True)
    chosen = (route_ids[:, :, None] == jnp.arange(experts_all, dtype=jnp.int32)).astype(jnp.int32)
    running = jnp.cumsum(chosen.reshape(2 * tok_rows, experts_all), axis=0).reshape(
        tok_rows, 2, experts_all
    )
    position = jnp.sum((running - 1) * chosen, axis=2)
    slot_ids = route_ids * capacity + position
    matches = (
        slot_ids[None, :, :] == jnp.arange(experts_all * capacity, dtype=jnp.int32)[:, None, None]
    )
    select_x = jnp.any(matches, axis=2).astype(jnp.float32)
    select_cot = jnp.sum(jnp.where(matches, route_weight[None], 0.0), axis=2)
    send_x = jnp.dot(
        select_x.astype(jnp.bfloat16), layer_in, preferred_element_type=jnp.float32
    ).astype(jnp.bfloat16)
    send_cot = jnp.dot(select_cot, out_cot.astype(jnp.float32), precision=highest).astype(
        jnp.bfloat16
    )
    send_x = send_x.reshape(experts_all, capacity, local_cols)
    send_cot = send_cot.reshape(experts_all, capacity, local_cols)
    recv_x, recv_cot = (
        lax.all_to_all(send_x, "sp", split_axis=0, concat_axis=0, tiled=True),
        lax.all_to_all(send_cot, "sp", split_axis=0, concat_axis=0, tiled=True),
    )
    head_dev = query.shape[1] // DK
    scaled_query = to_blocks(query, head_dev) * DK ** (-0.5)
    key_blk = to_blocks(key_in, head_dev)
    value_blk = to_blocks(value, head_dev)
    logit_blk = to_blocks(decay_logit, head_dev)
    cumulative = jnp.cumsum(jax.nn.log_sigmoid(logit_blk) / decay_temp, axis=2)
    span_log = cumulative[:, :, -1:, :]
    growth = jnp.exp(cumulative)
    shrink = jnp.exp(-cumulative)
    to_end = jnp.exp(span_log - cumulative)
    query_decayed = scaled_query * growth
    key_back = key_blk * shrink
    key_to_end = key_blk * to_end
    causal = jnp.tril(jnp.ones((BLOCK, BLOCK), dtype=bool))
    scores = jnp.where(
        causal, jnp.einsum("hncd,hnsd->hncs", query_decayed, key_back, precision=highest), 0.0
    )
    within = jnp.einsum("hncs,hnsv->hncv", scores, value_blk, precision=highest)
    block_decay = jnp.moveaxis(jnp.exp(span_log[:, :, 0, :]), 1, 0)
    block_update = jnp.moveaxis(
        jnp.einsum("hncd,hncv->hndv", key_to_end, value_blk, precision=highest), 1, 0
    )
    identity_pair = (
        jnp.ones((head_dev, DK), jnp.float32),
        jnp.zeros((head_dev, DK, DV), jnp.float32),
    )

    def advance(carry_pair, inputs):
        return (combine_spans(carry_pair, inputs), carry_pair)

    span_total, before_pairs = lax.scan(advance, identity_pair, (block_decay, block_update))
    entry_pair = prefix(span_total, "sp", combine_spans, identity_pair, False)
    entry_state = entry_pair[1]
    decay_before = jnp.moveaxis(before_pairs[0], 0, 1)
    block_state = decay_before[..., None] * entry_state[:, None] + jnp.moveaxis(
        before_pairs[1], 0, 1
    )
    span_end = span_total[0][..., None] * entry_state + span_total[1]
    outputs = within + jnp.einsum("hncd,hndv->hncv", query_decayed, block_state, precision=highest)
    mixer_out = from_blocks(outputs).astype(jnp.bfloat16)
    gate_mat, up_mat, down_mat = (gate_weight[0], up_weight[0], down_weight[0])
    gate_g, up_g, down_g, back_flat = expert_pass(
        recv_x.reshape(-1, local_cols), recv_cot.reshape(-1, local_cols), gate_mat, up_mat, down_mat
    )
    back_terms = back_flat.reshape(local_cols, experts_all, capacity)
    returned = lax.all_to_all(
        back_terms.astype(jnp.bfloat16), "sp", split_axis=1, concat_axis=1, tiled=True
    ).astype(back_terms.dtype)
    returned = returned.reshape(local_cols, experts_all * capacity)
    routed_sum = lax.dot_general(
        select_x,
        returned,
        (((0,), (1,)), ((), ())),
        precision=highest,
        preferred_element_type=jnp.float32,
    )
    mixed_cot = (out_cot.astype(jnp.float32) + routed_sum).astype(jnp.bfloat16)
    full_cot = lax.all_gather(mixed_cot, "tp", axis=1, tiled=True)
    mixer_cot = jnp.dot(full_cot, out_weight, preferred_element_type=jnp.float32)
    proj_grad = lax.psum_scatter(
        contract_rows(full_cot, mixer_out).astype(jnp.bfloat16),
        "sp",
        scatter_dimension=0,
        tiled=True,
    ).astype(jnp.float32)
    cot_blk = to_blocks(mixer_cot, head_dev)
    block_future = jnp.moveaxis(
        jnp.einsum("hncd,hncv->hndv", query_decayed, cot_blk, precision=highest), 1, 0
    )

    def retreat(carry_pair, inputs):
        return (combine_spans(carry_pair, inputs), carry_pair)

    span_back, after_pairs = lax.scan(
        retreat, identity_pair, (block_decay, block_future), reverse=True
    )
    beyond_pair = prefix(span_back, "sp", combine_spans, identity_pair, True)
    future_state = beyond_pair[1]
    decay_after = jnp.moveaxis(after_pairs[0], 0, 1)
    block_future_state = decay_after[..., None] * future_state[:, None] + jnp.moveaxis(
        after_pairs[1], 0, 1
    )
    cot_values = jnp.where(
        causal, jnp.einsum("hncv,hnsv->hncs", cot_blk, value_blk, precision=highest), 0.0
    )
    query_scaled_grad = growth * (
        jnp.einsum("hncv,hndv->hncd", cot_blk, block_state, precision=highest)
        + jnp.einsum("hncs,hnsd->hncd", cot_values, key_back, precision=highest)
    )
    key_part = shrink * jnp.einsum("hncs,hncd->hnsd", cot_values, query_decayed, precision=highest)
    key_grad = key_part + to_end * jnp.einsum(
        "hnsv,hndv->hnsd", value_blk, block_future_state, precision=highest
    )
    value_grad = jnp.einsum("hncs,hncv->hnsv", scores, cot_blk, precision=highest) + jnp.einsum(
        "hnsd,hndv->hnsv", key_to_end, block_future_state, precision=highest
    )
    decay_terms = (scaled_query * query_scaled_grad - key_blk * key_grad).reshape(
        head_dev, tok_rows, DK
    )
    tail_sum = jnp.flip(jnp.cumsum(jnp.flip(decay_terms, 1), axis=1), 1)
    beyond_term = jnp.sum(future_state * span_end, axis=2)
    log_grad = tail_sum + beyond_term[:, None, :]
    logit_flat = logit_blk.reshape(head_dev, tok_rows, DK)
    logit_grad = (
        (log_grad * jax.nn.sigmoid(-logit_flat) / decay_temp)
        .transpose(1, 0, 2)
        .reshape(tok_rows, head_dev * DK)
    )
    query_grad = from_blocks(query_scaled_grad * DK ** (-0.5))
    return (
        gate_g[None],
        up_g[None],
        down_g[None],
        proj_grad,
        query_grad,
        from_blocks(key_grad),
        from_blocks(value_grad),
        logit_grad,
    )


RING = 4
EXPERT_CUT = 5


def ring_place(index):
    return index + (index // 2) * (1 - 2 * (index % 2))


def remote(source, target, send_sem, recv_sem, device):
    return pltpu.make_async_remote_copy(
        src_ref=source,
        dst_ref=target,
        send_sem=send_sem,
        recv_sem=recv_sem,
        device_id=device,
        device_id_type=pl.DeviceIdType.MESH,
    )


def greet(devices):
    barrier = pltpu.get_barrier_semaphore()
    for device in devices:
        pl.semaphore_signal(
            barrier, inc=1, device_id=device, device_id_type=pl.DeviceIdType.MESH
        )
    pl.semaphore_wait(barrier, len(devices))


def arrived(sem, region):
    pltpu.make_async_copy(region, region, sem).wait()


class Place:
    def __init__(self):
        self.sp, self.tp = lax.axis_index("sp"), lax.axis_index("tp")
        self.z, self.core = self.tp // 2, self.tp % 2
        ring = ring_place(self.sp)
        self.at = [ring_place((ring + step) % RING) for step in range(RING)]
        self.right, self.across, self.left = [(self.at[s], self.tp) for s in (1, 2, 3)]
        self.pair = (self.sp, 2 * self.z + 1 - self.core)
        self.near = (self.sp, 2 * (self.z + 1 - 2 * (self.z % 2)) + self.core)
        self.far = (self.sp, 2 * (RING - 1 - self.z) + self.core)
        upper = self.z // 2
        folded = self.z + upper * (RING - 1 - 2 * self.z)
        self.inner = folded == 1
        self.end = folded == 0
        order = [folded, 1 - folded, 2, 3]
        self.slot = [o + upper * (RING - 1 - 2 * o) for o in order]


def expert_kernel(
    x_ref, cot_ref, small_ref, state_ref, gate_ref, up_ref, down_ref,
    gate_out, up_out, down_out, mixed_out, small_out, state_out,
    x_all, cot_all, gate_pre, up_pre, hidden, gate_cot, up_cot,
    pair_to, pair_from, parts, first_in, second_in, total, half_total, z_in,
    tiny_send, tiny_recv, zs, zr, ps, pr, qs, qr,
    bs, br, r1s, r1r, r2s, r2r, zts, ztr, ms, mr,
):
    here = Place()
    tok_rows, width = x_ref.shape
    lead = tok_rows * 4 // EXPERT_CUT
    tail = tok_rows - lead
    ins, alls = (x_ref, cot_ref), (x_all, cot_all)
    greet([here.right, here.across, here.left, here.near, here.far, here.pair])
    plain, guarded = [], []

    def go(source, target, send_sem, recv_sem, device):
        copy = remote(source, target, send_sem, recv_sem, device)
        copy.start()
        plain.append(copy)

    def go_if(cond, source, target, send_sem, recv_sem, device):
        copy = remote(source, target, send_sem, recv_sem, device)

        @pl.when(cond)
        def _():
            copy.start()

        guarded.append((cond, copy))

    def cols(slot, core):
        return pl.ds(pl.multiple_of((2 * here.slot[slot] + core) * width, width), width)

    def piece(a, part, slot, core=None):
        core = here.core if core is None else core
        if part == 0:
            return alls[a].at[here.sp, pl.ds(0, lead), cols(slot, core)]
        return alls[a].at[:, pl.ds(lead, tail), cols(slot, core)]

    def own_rows(a, start, count):
        return ins[a].at[pl.ds(start, count), :]

    def z_start(a, part):
        source = own_rows(a, 0, lead) if part == 0 else piece(a, 1, 0)
        target = piece(a, part, 0)
        go(source, target, zs.at[a, part, 0], zr.at[a, part, 0], here.near)
        go_if(here.inner, source, target, zs.at[a, part, 1], zr.at[a, part, 1], here.far)

    def z_relay(a, part, slot):
        region = piece(a, part, slot)
        arrived(zr.at[a, part, slot - 1], region)
        if slot == 1:
            go_if(here.inner, region, region, zs.at[a, part, 2], zr.at[a, part, 2], here.far)
        else:
            go_if(
                here.inner, region, region, zs.at[a, part, slot + 1], zr.at[a, part, slot - 1],
                here.near,
            )
        if part == 0:
            pair_send(a, slot, 0)
        else:
            go(region, region, qs.at[a, slot, 4], qr.at[a, slot, 4], here.pair)

    def bounds(part, h):
        start, count = (0, lead) if part == 0 else (lead, tail)
        return start + h * (count // 2), count // 2

    def ring_region(a, unit, step, h):
        slot, part = unit
        start, count = bounds(part, h)
        return alls[a].at[here.at[step], pl.ds(start, count), cols(slot, here.core)]

    def number(unit):
        return unit[0] + 4 * unit[1]

    def ring_send(a, unit):
        slot, part = unit
        n = number(unit)
        for h, right_first in ((0, True), (1, False)):
            pass
        for i, (h, device) in enumerate(
            ((0, here.right), (1, here.right), (0, here.left), (1, here.left))
        ):
            start, count = bounds(part, h)
            source = own_rows(a, start, count) if slot == 0 else ring_region(a, unit, 0, h)
            copy = remote(source, ring_region(a, unit, 0, h), ps.at[a, n, i], pr.at[a, n, i], device)
            plain.append(copy)
        right0, right1, left0, left1 = plain[-4:]
        for copy in (right0, left1, right1, left0):
            copy.start()

    def ring_forward(a, unit):
        n = number(unit)
        region = ring_region(a, unit, 3, 0)
        arrived(pr.at[a, n, 0], region)
        go(region, region, ps.at[a, n, 4], pr.at[a, n, 4], here.right)
        region = ring_region(a, unit, 1, 1)
        arrived(pr.at[a, n, 3], region)
        go(region, region, ps.at[a, n, 5], pr.at[a, n, 5], here.left)

    def ring_finish(a, unit):
        n = number(unit)
        arrived(pr.at[a, n, 1], ring_region(a, unit, 3, 1))
        arrived(pr.at[a, n, 2], ring_region(a, unit, 1, 0))
        arrived(pr.at[a, n, 4], ring_region(a, unit, 2, 0))
        arrived(pr.at[a, n, 5], ring_region(a, unit, 2, 1))
        if unit[1] == 0:
            for step in (1, 3, 2):
                pair_send(a, unit[0], step)
        else:
            z_start(a, 1)
            region = piece(a, 1, 0)
            go(region, region, qs.at[a, 0, 4], qr.at[a, 0, 4], here.pair)

    def pair_region(a, slot, step, core):
        return alls[a].at[here.at[step], pl.ds(0, lead), cols(slot, core)]

    def pair_send(a, slot, step):
        region = pair_region(a, slot, step, here.core)
        source = own_rows(a, 0, lead) if slot == 0 and step == 0 else region
        go(source, region, qs.at[a, slot, step], qr.at[a, slot, step], here.pair)

    def pair_wait(a, part):
        for slot in range(RING):
            if part == 0:
                for step in range(RING):
                    arrived(qr.at[a, slot, step], pair_region(a, slot, step, 1 - here.core))
            else:
                arrived(qr.at[a, slot, 4], piece(a, 1, slot, 1 - here.core))

    for a in range(2):
        z_start(a, 0)
    ring_send(0, (0, 0))
    for ref, out, i in ((small_ref, small_out, 0), (state_ref, state_out, 1)):
        for step, device in ((1, here.right), (3, here.left), (2, here.across)):
            go(
                ref, out.at[here.sp], tiny_send.at[i, step - 1], tiny_recv.at[i, 3 - step], device
            )
    ring_send(0, (0, 1))
    ring_send(1, (0, 1))
    for a in range(2):
        alls[a][here.sp, :, cols(0, here.core)] = ins[a][...]
        pair_send(a, 0, 0)
    small_out[here.sp] = small_ref[...]
    state_out[here.sp] = state_ref[...]
    z_relay(0, 0, 1)
    ring_send(0, (1, 0))
    ring_forward(0, (0, 0))
    ring_forward(0, (0, 1))
    ring_forward(1, (0, 1))
    z_relay(0, 0, 2)
    ring_send(0, (2, 0))
    ring_forward(0, (1, 0))
    ring_finish(0, (0, 0))
    z_relay(0, 0, 3)
    ring_send(0, (3, 0))
    ring_forward(0, (2, 0))
    ring_finish(0, (1, 0))
    z_relay(1, 0, 1)
    ring_send(1, (0, 0))
    ring_send(1, (1, 0))
    ring_forward(0, (3, 0))
    ring_finish(0, (2, 0))
    z_relay(1, 0, 2)
    ring_send(1, (2, 0))
    ring_finish(0, (0, 1))
    z_relay(1, 0, 3)
    ring_send(1, (3, 0))
    ring_finish(1, (0, 1))
    ring_forward(1, (0, 0))
    ring_finish(0, (3, 0))
    pair_wait(0, 0)

    def forward_rows(s, start, count):
        rows = pl.ds(start, count)
        block = x_all[s, rows, :]
        gate_pre[s, rows, :] = contract_cols(block, gate_ref[...])
        up_pre[s, rows, :] = contract_cols(block, up_ref[...])

    half = lead // 2
    steps = [
        lambda: ring_forward(1, (1, 0)),
        lambda: z_relay(0, 1, 1),
        lambda: ring_finish(1, (0, 0)),
        lambda: z_relay(0, 1, 2),
        lambda: ring_forward(1, (2, 0)),
        lambda: ring_finish(1, (1, 0)),
        lambda: z_relay(0, 1, 3),
        lambda: ring_forward(1, (3, 0)),
    ]
    for i in range(8):
        forward_rows(i // 2, (i % 2) * half, half)
        steps[i]()
    for s in range(RING):
        for step in (1, 2, 3):
            pass
    for step in (1, 2, 3):
        arrived(tiny_recv.at[0, step - 1], small_out.at[here.at[step]])
        arrived(tiny_recv.at[1, step - 1], state_out.at[here.at[step]])
    ring_finish(1, (2, 0))
    z_relay(1, 1, 1)
    pair_wait(0, 1)
    for s in range(RING):
        forward_rows(s, lead, tail)
    z_relay(1, 1, 2)
    z_relay(1, 1, 3)
    ring_finish(1, (3, 0))
    pair_wait(1, 0)

    pick = (
        lax.broadcasted_iota(jnp.int32, (small_ref.shape[0], 128), 0) == here.sp
    ).astype(jnp.float32)

    def second_rows(s, start, count):
        rows = pl.ds(start, count)
        weight = lax.dot_general(
            small_out[s, :, pl.ds(0, tok_rows)][:, start : start + count],
            pick,
            (((0,), (0,)), ((), ())),
            precision=lax.Precision.HIGHEST,
            preferred_element_type=jnp.float32,
        )
        weight = jnp.concatenate([weight] * (width // 128), axis=1)
        hidden_cot = contract_cols(cot_all[s, rows, :], down_ref[...]) * weight
        gp, upp = gate_pre[s, rows, :], up_pre[s, rows, :]
        sig = 1.0 / (1.0 + jnp.exp(-gp))
        active = gp * sig
        hidden[s, rows, :] = (active * upp * weight).astype(jnp.bfloat16)
        up_cot[s, rows, :] = (hidden_cot * active).astype(jnp.bfloat16)
        gate_cot[s, rows, :] = (hidden_cot * upp * sig * (1.0 + gp * (1.0 - sig))).astype(
            jnp.bfloat16
        )

    for i in range(8):
        second_rows(i // 2, (i % 2) * half, half)
    pair_wait(1, 1)
    for s in range(RING):
        second_rows(s, lead, tail)

    pieces, wide = parts.shape[0], parts.shape[3]
    split = tok_rows // 2
    per = width // wide

    def back_cols(k, core):
        at = (2 * (k // per) + core) * width + (k % per) * wide
        return pl.ds(pl.multiple_of(at, wide), wide)

    def partial(k, step, core):
        c = back_cols(k, core)
        s = here.at[step]
        return jnp.dot(
            gate_cot[s], gate_ref[:, c], preferred_element_type=jnp.float32
        ) + jnp.dot(up_cot[s], up_ref[:, c], preferred_element_type=jnp.float32)

    ring_order = (2, 1, 3, 0)

    def pair_part(k):
        for step in ring_order:
            pair_to[k, step] = partial(k, step, 1 - here.core).astype(jnp.bfloat16)
            go(
                pair_to.at[k, step], pair_from.at[k, step], bs.at[k, step], br.at[k, step], here.pair
            )

    top, bottom = pl.ds(0, split), pl.ds(split, split)

    def own_part(k):
        for step in ring_order:
            mine = partial(k, step, here.core)
            arrived(br.at[k, step], pair_from.at[k, step])
            parts[k, step] = (mine + pair_from[k, step].astype(jnp.float32)).astype(jnp.bfloat16)
            if step == 2:
                go(parts.at[k, 2, top], first_in.at[k, 0], r1s.at[k, 0], r1r.at[k, 0], here.right)
                go(parts.at[k, 2, bottom], first_in.at[k, 1], r1s.at[k, 1], r1r.at[k, 1], here.left)
            if step == 1:
                go(
                    parts.at[k, 1, bottom], second_in.at[k, 0, bottom],
                    r2s.at[k, 0], r2r.at[k, 0], here.right,
                )
            if step == 3:
                go(
                    parts.at[k, 3, top], second_in.at[k, 1, top],
                    r2s.at[k, 1], r2r.at[k, 1], here.left,
                )

    def add_to(ref, other):
        ref[...] = (ref[...].astype(jnp.float32) + other.astype(jnp.float32)).astype(jnp.bfloat16)

    def ring_relay(k):
        arrived(r1r.at[k, 0], first_in.at[k, 0])
        add_to(parts.at[k, 1, top], first_in[k, 0])
        go(
            parts.at[k, 1, top], second_in.at[k, 0, top], r2s.at[k, 2], r2r.at[k, 2], here.right
        )
        arrived(r1r.at[k, 1], first_in.at[k, 1])
        add_to(parts.at[k, 3, bottom], first_in[k, 1])
        go(
            parts.at[k, 3, bottom], second_in.at[k, 1, bottom],
            r2s.at[k, 3], r2r.at[k, 3], here.left,
        )

    def ring_total(k):
        arrived(r2r.at[k, 0], second_in.at[k, 0, bottom])
        arrived(r2r.at[k, 1], second_in.at[k, 1, top])
        arrived(r2r.at[k, 2], second_in.at[k, 0, top])
        arrived(r2r.at[k, 3], second_in.at[k, 1, bottom])
        total[k] = (
            parts[k, 0].astype(jnp.float32)
            + second_in[k, 0].astype(jnp.float32)
            + second_in[k, 1].astype(jnp.float32)
        ).astype(jnp.bfloat16)
        go_if(here.end, total.at[k], z_in.at[k, 0], zts.at[k, 0], ztr.at[k, 0], here.near)

    def line_middle(k):
        copy = remote(half_total.at[k], z_in.at[k, 1], zts.at[k, 1], ztr.at[k, 1], here.far)

        @pl.when(here.inner)
        def _():
            arrived(ztr.at[k, 0], z_in.at[k, 0])
            half_total[k] = (
                total[k].astype(jnp.float32) + z_in[k, 0].astype(jnp.float32)
            ).astype(jnp.bfloat16)
            copy.start()

        guarded.append((here.inner, copy))

    def line_total(k):
        c = back_cols(k, here.core)
        region = mixed_out.at[:, c]
        copy = remote(region, region, ms.at[k, 0], mr.at[k, 0], here.near)

        @pl.when(here.inner)
        def _():
            arrived(ztr.at[k, 1], z_in.at[k, 1])
            mixed_out[:, c] = (
                cot_all[here.sp, :, c].astype(jnp.float32)
                + (half_total[k].astype(jnp.float32) + z_in[k, 1].astype(jnp.float32))
            ).astype(jnp.bfloat16)
            copy.start()

        guarded.append((here.inner, copy))

        @pl.when(here.end)
        def _():
            arrived(mr.at[k, 0], region)

        go(region, region, ms.at[k, 1], mr.at[k, 1], here.pair)

    features = gate_ref.shape[1]
    blocks = features // width

    def weight_grad(n):
        which, j = n // blocks, n % blocks
        left, right, out = (
            (gate_cot, x_all, gate_out), (up_cot, x_all, up_out), (hidden, cot_all, down_out)
        )[which]
        c = pl.ds(j * width, width)
        rows = RING * tok_rows
        out[:, c] = contract_rows(
            left[...].reshape(rows, width), right[:, :, c].reshape(rows, width)
        )

    grads = list(range(3 * blocks))

    def some_grads(count):
        for _ in range(min(count, len(grads))):
            weight_grad(grads.pop(0))

    lanes = []
    pair_part(0)
    for k in range(pieces + 5):
        if k + 1 < pieces:
            pair_part(k + 1)
        if k < pieces:
            own_part(k)
        some_grads(-(-3 * blocks // (pieces + 4)))
        if 0 <= k - 1 < pieces:
            ring_relay(k - 1)
        if 0 <= k - 2 < pieces:
            ring_total(k - 2)
        if 0 <= k - 3 < pieces:
            line_middle(k - 3)
        if 0 <= k - 4 < pieces:
            line_total(k - 4)
    some_grads(3 * blocks)
    for k in range(pieces):
        arrived(mr.at[k, 1], mixed_out.at[:, back_cols(k, 1 - here.core)])
    for copy in plain:
        copy.wait_send()
    for cond, copy in guarded:
        @pl.when(cond)
        def _():
            copy.wait_send()


def expert_stage(x, cot, small, state, gate, up, down):
    tok_rows, width = x.shape
    hidden_dev, features = gate.shape
    pieces, wide = 4, 2 * features // (2 * RING * 2)
    vmem = pl.BlockSpec(memory_space=pltpu.VMEM)
    dma = pltpu.SemaphoreType.DMA
    f32, bf16 = jnp.float32, jnp.bfloat16
    full = (RING, tok_rows, features)
    acts = (RING, tok_rows, hidden_dev)
    block = (tok_rows, wide)
    return pl.pallas_call(
        expert_kernel,
        out_shape=[jax.ShapeDtypeStruct((hidden_dev, features), f32)] * 3 + [
            jax.ShapeDtypeStruct((tok_rows, features), bf16),
            jax.ShapeDtypeStruct((RING,) + small.shape, small.dtype),
            jax.ShapeDtypeStruct((RING,) + state.shape, state.dtype),
        ],
        in_specs=[vmem] * 7,
        out_specs=[vmem] * 6,
        scratch_shapes=[
            pltpu.VMEM(full, bf16), pltpu.VMEM(full, bf16),
            pltpu.VMEM(acts, f32), pltpu.VMEM(acts, f32),
            pltpu.VMEM(acts, bf16), pltpu.VMEM(acts, bf16), pltpu.VMEM(acts, bf16),
            pltpu.VMEM((pieces, RING) + block, bf16), pltpu.VMEM((pieces, RING) + block, bf16),
            pltpu.VMEM((pieces, RING) + block, bf16),
            pltpu.VMEM((pieces, 2, tok_rows // 2, wide), bf16),
            pltpu.VMEM((pieces, 2) + block, bf16),
            pltpu.VMEM((pieces,) + block, bf16), pltpu.VMEM((pieces,) + block, bf16),
            pltpu.VMEM((pieces, 2) + block, bf16),
            dma((2, 3)), dma((2, 3)),
            dma((2, 2, 5)), dma((2, 2, 3)),
            dma((2, 5, 6)), dma((2, 5, 6)),
            dma((2, 4, 5)), dma((2, 4, 5)),
            dma((pieces, 4)), dma((pieces, 4)),
            dma((pieces, 2)), dma((pieces, 2)),
            dma((pieces, 4)), dma((pieces, 4)),
            dma((pieces, 2)), dma((pieces, 2)),
            dma((pieces, 2)), dma((pieces, 2)),
        ],
        compiler_params=pltpu.CompilerParams(
            collective_id=0, has_side_effects=True, vmem_limit_bytes=60 << 20
        ),
        name="expert_stage",
    )(x, cot, small, state, gate, up, down)


def exchange_kernel(x_ref, out_ref, send_sem, recv_sem):
    here = Place()
    devices = (here.right, here.across, here.left)
    greet(devices)
    sends = []
    for step in (1, 3, 2):
        copy = remote(
            x_ref.at[here.at[step]], out_ref.at[here.sp],
            send_sem.at[step - 1], recv_sem.at[3 - step], devices[step - 1],
        )
        copy.start()
        sends.append(copy)
    out_ref[here.sp] = x_ref[here.sp]
    for step in (1, 2, 3):
        arrived(recv_sem.at[step - 1], out_ref.at[here.at[step]])
    for copy in sends:
        copy.wait_send()


def exchange(x, number):
    vmem = pl.BlockSpec(memory_space=pltpu.VMEM)
    dma = pltpu.SemaphoreType.DMA
    return pl.pallas_call(
        exchange_kernel,
        out_shape=jax.ShapeDtypeStruct(x.shape, x.dtype),
        in_specs=[vmem],
        out_specs=vmem,
        scratch_shapes=[dma((3,)), dma((3,))],
        compiler_params=pltpu.CompilerParams(collective_id=number, has_side_effects=True),
        name="exchange" + str(number),
    )(x)


def ring_local(
    layer_in, out_cot, route_ids, route_probs, group_prob, gate_weight, up_weight,
    down_weight, out_weight, query, key_in, value, decay_logit,
):
    tok_rows, local_cols = layer_in.shape
    experts_all = lax.axis_size("sp")
    here = lax.axis_index("sp")
    route_weight = group_prob[:, None] * route_probs / jnp.sum(route_probs, axis=1, keepdims=True)
    table = jnp.sum(
        jnp.where(
            route_ids[None] == jnp.arange(experts_all, dtype=jnp.int32)[:, None, None],
            route_weight[None],
            0.0,
        ),
        axis=2,
    )
    head_dev = query.shape[1] // DK

    def heads(tensor):
        return tensor.astype(jnp.float32).reshape(tok_rows, head_dev, -1).transpose(1, 0, 2)

    def flat(tensor):
        return tensor.transpose(1, 0, 2).reshape(tok_rows, -1)

    def product(spec, a, b):
        return jnp.einsum(spec, a, b, precision=highest)

    scaled_query = heads(query) * DK ** (-0.5)
    key_h, value_h, logit_h = heads(key_in), heads(value), heads(decay_logit)
    causal = jnp.tril(jnp.ones((tok_rows, tok_rows), dtype=bool))
    ones = causal.astype(jnp.float32)
    cumulative = product("cs,hsd->hcd", ones, jax.nn.log_sigmoid(logit_h) / decay_temp)
    span_log = cumulative[:, -1:, :]
    growth, shrink = jnp.exp(cumulative), jnp.exp(-cumulative)
    to_end = jnp.exp(span_log - cumulative)
    query_decayed, key_back, key_to_end = scaled_query * growth, key_h * shrink, key_h * to_end
    span_decay = jnp.exp(span_log[:, 0, :])
    span_state = product("hcd,hcv->hdv", key_to_end, value_h)
    lanes = -(-max(tok_rows, head_dev * DK) // 128) * 128
    small = jnp.zeros((8, lanes), jnp.float32)
    small = small.at[:experts_all, :tok_rows].set(table)
    small = small.at[experts_all, : head_dev * DK].set(span_decay.reshape(-1))
    gate_g, up_g, down_g, full_mixed, smalls, states = expert_stage(
        layer_in, out_cot, small, span_state.astype(jnp.bfloat16).reshape(head_dev * DK, DV),
        gate_weight[0], up_weight[0], down_weight[0],
    )
    decays = smalls[:, experts_all, : head_dev * DK].reshape(RING, head_dev, DK, 1)
    states = states.astype(jnp.float32).reshape(RING, head_dev, DK, DV)
    entry_state = jnp.zeros((head_dev, DK, DV), jnp.float32)
    for s in range(RING - 1):
        entry_state = jnp.where(s < here, entry_state * decays[s] + states[s], entry_state)
    span_end = span_decay[..., None] * entry_state + span_state
    scores = jnp.where(causal, product("hcd,hsd->hcs", query_decayed, key_back), 0.0)
    outputs = product("hcs,hsv->hcv", scores, value_h) + product(
        "hcd,hdv->hcv", query_decayed, entry_state
    )
    mixer_out = flat(outputs).astype(jnp.bfloat16)
    mixer_cot = jnp.dot(full_mixed, out_weight, preferred_element_type=jnp.float32)
    proj_parts = contract_rows(full_mixed, mixer_out).astype(jnp.bfloat16)
    proj_parts = exchange(proj_parts.reshape(RING, -1, proj_parts.shape[1]), 1)
    proj_grad = jnp.sum(proj_parts.astype(jnp.float32), axis=0)
    cot_h = heads(mixer_cot)
    span_future = product("hcd,hcv->hdv", query_decayed, cot_h)
    futures = exchange(
        jnp.broadcast_to(
            span_future.astype(jnp.bfloat16).reshape(1, head_dev * DK, DV), (RING, head_dev * DK, DV)
        ),
        2,
    )
    futures = futures.astype(jnp.float32).reshape(RING, head_dev, DK, DV)
    future_state = jnp.zeros((head_dev, DK, DV), jnp.float32)
    for s in range(RING - 1, 0, -1):
        future_state = jnp.where(s > here, future_state * decays[s] + futures[s], future_state)
    cot_values = jnp.where(causal, product("hcv,hsv->hcs", cot_h, value_h), 0.0)
    query_scaled_grad = growth * (
        product("hcv,hdv->hcd", cot_h, entry_state) + product("hcs,hsd->hcd", cot_values, key_back)
    )
    key_grad = shrink * product("hcs,hcd->hsd", cot_values, query_decayed) + to_end * product(
        "hsv,hdv->hsd", value_h, future_state
    )
    value_grad = product("hcs,hcv->hsv", scores, cot_h) + product(
        "hsd,hdv->hsv", key_to_end, future_state
    )
    decay_terms = scaled_query * query_scaled_grad - key_h * key_grad
    tail_sum = product("cs,hcd->hsd", ones, decay_terms)
    log_grad = tail_sum + jnp.sum(future_state * span_end, axis=2)[:, None, :]
    logit_grad = flat(log_grad * jax.nn.sigmoid(-logit_h) / decay_temp)
    return (
        gate_g[None], up_g[None], down_g[None], proj_grad,
        flat(query_scaled_grad * DK ** (-0.5)), flat(key_grad), flat(value_grad), logit_grad,
    )


def solution(mesh):
    in_specs = (
        P("sp", "tp"),
        P("sp", "tp"),
        P("sp", None),
        P("sp", None),
        P("sp"),
        P("sp", "tp", None),
        P("sp", "tp", None),
        P("sp", "tp", None),
        P(None, "tp"),
        P("sp", "tp"),
        P("sp", "tp"),
        P("sp", "tp"),
        P("sp", "tp"),
    )
    out_specs = (
        P("sp", "tp", None),
        P("sp", "tp", None),
        P("sp", "tp", None),
        P("sp", "tp"),
        P("sp", "tp"),
        P("sp", "tp"),
        P("sp", "tp"),
        P("sp", "tp"),
    )
    rows = 4 // mesh.shape["sp"]
    body = ring_local if rows * 4 == 4 and mesh.shape["tp"] == 8 else local
    return jax.shard_map(body, mesh=mesh, in_specs=in_specs, out_specs=out_specs, check_vma=False)
```

time: 257 us -> 172 us (0.67)
  waiting for transfers between devices: 76.6 us -> 0 us
  Pallas kernels: 72.4 us -> 139 us
  matrix products: 46.1 us -> 12 us
  other arithmetic: 21 us -> 3.53 us
  between operations: 14.9 us -> 1.01 us
  local copies, waits for them, and re-layouts: 20.6 us -> 15.6 us
  starting transfers between devices: 4.46 us -> 0 us
    pallas_call x2 -> x3, Pallas kernels: 72.4 us -> 139 us  [the longest x1 115 us: expert_stage(): pl.pallas_call(expert_kernel, out_shape=[jax.ShapeDtypeStruct((hidden_dev...]
    reduce_scatter x2 -> x0, waiting for transfers between devices: 66.5 us -> none  [the longest x1 55.5 us: ring_local(): back_terms = lax.psum_scatter(back, 'tp', scatter_dimension=1, tiled=True)]
    dot_general x19 -> x13, matrix products: 30.4 us -> 8.19 us  [product(): return jnp.einsum(spec, a, b, precision=highest)]
    dot_general x4 -> x1, matrix products: 13.6 us -> 1.71 us  [contract_rows(): lax.dot_general(left_mat, right_mat, (((0,), (0,)), ((), ())), preferred_...]
    all_gather x1 -> x0, waiting for transfers between devices: 9.99 us -> none  [ring_local(): full_mixed = lax.all_gather(mixed_cot, 'tp', axis=1, tiled=True)]
    unnamed x150 -> x35, local copies, waits for them, and re-layouts: 3.22 us -> 11.5 us
    unnamed x8 -> x0, other arithmetic: 6.51 us -> none
    convert_element_type x6 -> x0, other arithmetic: 6.38 us -> none  [the longest x1 1.78 us: ring_local(): proj_grad = lax.psum_scatter(contract_rows(full_mixed, mixer_out).astype(...]
  transfers between devices with their start and end apart: 4 -> 0, of which waited for: 3 -> 0; matrix products, arithmetic and copies ran while one was open for 17% -> 0% of each run, Pallas kernels for 0% -> 0%
where the time goes in v1:
time: 172 us; the launch traced here: 171 us
  Pallas kernels  139 us (81%)
  local copies, waits for them, and re-layouts  15.6 us (9%)
  matrix products  12 us (7%)
  other arithmetic  3.53 us (2%)
    pallas_call x1, Pallas kernels, expert_stage(): pl.pallas_call(expert_kernel, out_shape=[jax.ShapeDtypeStruct((hidden_dev...  115 us
    pallas_call x2, Pallas kernels, exchange(): pl.pallas_call(exchange_kernel, out_shape=jax.ShapeDtypeStruct(x.shape, x...  24.1 us
    unnamed x35, local copies, waits for them, and re-layouts  11.5 us
    dot_general x13, matrix products, product(): return jnp.einsum(spec, a, b, precision=highest)  8.19 us

profile of v1, /device:TPU:0, one launch (start us, length us, event | category | flops | bytes accessed | tf_op | source)
XLA Modules:
  0.0 171.3 jit_solution(15843404505504136117)
XLA Ops:
  0.7 1.1 copy.46
  1.8 0.4 fusion.3
  2.4 1.0 copy.47
  3.4 1.8 %fusion.53 = (bf16[2,64,128]{2,1,0:T(8,128)(2,1)}, f32[2,64,128]{2,1,0:T(8,128)S(1)}) fusion(f32[2,320,64]{1,2,0:T(8,128)S(1)} %bitcast.152, f32[2,64]{1,0:T(2,128)S(1)} %get-tuple-element.68, f32[2,64,320]{2,1,0:T(8,128)S(1)} %fusion.3, bf16[320,256]{1,0:T(8,128)(2,1)} %param.28), kind=kOutput, calls=%fused_computation.85 | convolution fusion | flops 31555584 | bytes 590336 | tf_op jit(solution)/shard_map/hcd,hcv->hdv/dot_general | solution.py:816
  5.6 0.6 copy-done.9
  6.2 115.0 %expert_stage.1 = (f32[256,2048]{1,0:T(8,128)}, f32[256,2048]{1,0:T(8,128)}, f32[256,2048]{1,0:T(8,128)}, bf16[320,2048]{1,0:T(8,128)(2,1)}, f32[4,8,384]{2,1,0:T(8,128)}, /*index=5*/bf16[4,128,128]{2,1,0:T(8,128)(2,1)}) custom-call(bf16[320,256]{1,0:T(8,128)(2,1)} %x_ref.1, bf16[320,256]{1,0:T(8,128)(2,1)} %cot_ref.1, f32[8,384]{1,0:T(8,128)} %copy-done.9, ...), custom_call_target="tpu_custom_call" | custom-call | tf_op jit(solution)/shard_map/expert_stage/pallas_call | solution.py:722
  121.3 1.9 %convolution_bitcast_fusion = f32[40,2,8,128]{3,2,1,0:T(8,128)S(1)} fusion(bf16[320,2048]{1,0:T(8,128)(2,1)} %get-tuple-element.41, bf16[2048,256]{1,0:T(8,128)(2,1)S(1)} %copy-done), kind=kOutput, calls=%fused_computation.6 | convolution fusion | flops 335544320 | bytes 2686976 | tf_op jit(solution)/shard_map/dot_general | solution.py:848
  123.6 0.7 broadcast_in_dim.59.x_ref
  124.3 7.1 %exchange2.1 = bf16[4,128,128]{2,1,0:T(8,128)(2,1)} custom-call(bf16[4,128,128]{2,1,0:T(8,128)(2,1)} %broadcast_in_dim.59.x_ref), custom_call_target="tpu_custom_call" | custom-call | tf_op jit(solution)/shard_map/exchange2/pallas_call | solution.py:780
  131.4 0.8 fusion.52
  132.2 0.7 multiply_reduce_fusion.1
  133.6 0.4 convolution_select_fusion.1
  134.1 0.6 fusion.39
  135.2 1.1 bitcast_add_fusion
  136.8 0.8 copy.56
  137.6 0.6 convolution_select_fusion
  138.3 1.1 fusion.5
  139.3 0.5 fusion
  139.9 0.7 copy.101
  140.6 1.7 copy.54
  142.3 0.8 copy.55
  143.1 0.4 fusion.31
  143.5 0.5 fusion.2
  144.0 0.4 copy-done.13
  144.4 1.7 %convolution_convert_fusion = bf16[2048,256]{1,0:T(8,128)(2,1)} fusion(bf16[320,2048]{1,0:T(8,128)(2,1)S(1)} %copy-done.13, bf16[2,40,8,128]{3,2,1,0:T(8,128)(2,1)S(1)} %fusion.2), kind=kOutput, calls=%fused_computation | convolution fusion | flops 336068608 | bytes 2523136 | tf_op jit(solution)/shard_map/dot_general | solution.py:48
  146.2 16.9 %exchange1.1 = bf16[4,512,256]{2,1,0:T(8,128)(2,1)} custom-call(bf16[4,512,256]{2,1,0:T(8,128)(2,1)} %bitcast.165), custom_call_target="tpu_custom_call" | custom-call | tf_op jit(solution)/shard_map/exchange1/pallas_call | solution.py:780
  163.1 2.2 %convert_reduce_fusion = f32[512,256]{1,0:T(8,128)} fusion(bf16[4,512,256]{2,1,0:T(8,128)(2,1)} %exchange1.1), kind=kLoop, calls=%fused_computation.1 | loop fusion | flops 917504 | bytes 1572864 | tf_op jit(solution)/shard_map/reduce_sum | solution.py:851
  165.3 1.3 copy.106
  166.6 1.0 copy-done.3
  167.7 1.3 copy.107
  169.0 1.0 copy-done.2
  170.0 1.3 copy.108
  (48 shorter events, 2.7 us)
Async XLA Ops:
  0.6 120.7 %copy-start = (bf16[2048,256]{1,0:T(8,128)(2,1)S(1)}, bf16[2048,256]{1,0:T(8,128)(2,1)}, u32[]{:S(2)}) copy-start(bf16[2048,256]{1,0:T(8,128)(2,1)} %param.25) | copy-start | bytes 3145732
  0.6 4.7 %copy-start.10 = (f32[320,2]{0,1:T(2,128)S(1)}, f32[320,2]{0,1:T(2,128)}, u32[]{:S(2)}) copy-start(f32[320,2]{0,1:T(2,128)} %param.20) | copy-start | bytes 7684
  0.7 4.7 %copy-start.12 = (f32[320]{0:T(512)S(1)}, f32[320]{0:T(512)}, u32[]{:S(2)}) copy-start(f32[320]{0:T(512)} %param.21) | copy-start | bytes 3844
  0.7 4.7 %copy-start.11 = (s32[320,2]{0,1:T(2,128)S(1)}, s32[320,2]{0,1:T(2,128)}, u32[]{:S(2)}) copy-start(s32[320,2]{0,1:T(2,128)} %param.19) | copy-start | bytes 7684
  5.6 0.6 copy-start.9
  121.3 1.9 %copy-start.8 = (bf16[320,128]{1,0:T(8,128)(2,1)S(1)}, bf16[320,128]{1,0:T(8,128)(2,1)}, u32[]{:S(2)}) copy-start(bf16[320,128]{1,0:T(8,128)(2,1)} %param.26) | copy-start | bytes 245764
  121.3 12.0 %copy-start.7 = (bf16[4,128,128]{2,1,0:T(8,128)(2,1)S(1)}, bf16[4,128,128]{2,1,0:T(8,128)(2,1)}, u32[]{:S(2)}) copy-start(bf16[4,128,128]{2,1,0:T(8,128)(2,1)} %get-tuple-element.43) | copy-start | bytes 393220
  123.2 10.4 %copy-start.1 = (bf16[320,256]{1,0:T(8,128)(2,1)S(1)}, bf16[320,256]{1,0:T(8,128)(2,1)}, u32[]{:S(2)}) copy-start(bf16[320,256]{1,0:T(8,128)(2,1)} %param.28) | copy-start | bytes 491524
  133.6 1.7 copy-start.5
  139.3 4.2 %copy-start.6 = (f32[2,64,128]{2,1,0:T(8,128)S(1)}, f32[2,64,128]{2,1,0:T(8,128)}, u32[]{:S(2)}) copy-start(f32[2,64,128]{2,1,0:T(8,128)} %copy-done.5) | copy-start | bytes 196612
  143.1 1.3 copy-start.13
  146.2 19.2 %copy-start.4 = (f32[256,2048]{1,0:T(8,128)S(1)}, f32[256,2048]{1,0:T(8,128)}, u32[]{:S(2)}) copy-start(f32[256,2048]{1,0:T(8,128)} %get-tuple-element.38) | copy-start | bytes 6291460
  165.3 2.3 %copy-start.3 = (f32[256,2048]{1,0:T(8,128)S(1)}, f32[256,2048]{1,0:T(8,128)}, u32[]{:S(2)}) copy-start(f32[256,2048]{1,0:T(8,128)} %get-tuple-element.39) | copy-start | bytes 6291460
  167.7 2.3 %copy-start.2 = (f32[256,2048]{1,0:T(8,128)S(1)}, f32[256,2048]{1,0:T(8,128)}, u32[]{:S(2)}) copy-start(f32[256,2048]{1,0:T(8,128)} %get-tuple-element.40) | copy-start | bytes 6291460

commit v2 on v1

--- a/solution.py
+++ b/solution.py
@@ -267,6 +267,147 @@
 
 RING = 4
 EXPERT_CUT = 5
+PIECES = 8
+GATHER_ORDER = (
+    ("rs", 1, 4),
+    ("rs", 0, 4),
+    ("zs", 0, 0),
+    ("zs", 1, 0),
+    ("rs", 0, 0),
+    ("rf", 0, 4, 1),
+    ("rf", 0, 4, 0),
+    ("prep",),
+    ("rf", 1, 4, 1),
+    ("rf", 1, 4, 0),
+    ("zr", 0, 0, 1),
+    ("rs", 1, 0),
+    ("zr", 0, 0, 2),
+    ("zr", 1, 0, 1),
+    ("rd", 0, 4),
+    ("zr", 0, 0, 3),
+    ("mixf",),
+    ("rd", 1, 4),
+    ("rf", 0, 1, 1),
+    ("fx", 0),
+    ("rf", 0, 1, 0),
+    ("rf", 0, 0, 1),
+    ("zr", 0, 1, 2),
+    ("rf", 0, 2, 1),
+    ("rf", 0, 0, 0),
+    ("zr", 0, 1, 1),
+    ("rf", 0, 2, 0),
+    ("zr", 1, 0, 2),
+    ("rf", 0, 3, 1),
+    ("rf", 0, 3, 0),
+    ("zr", 0, 1, 3),
+    ("rf", 1, 0, 1),
+    ("rf", 1, 0, 0),
+    ("rf", 1, 1, 1),
+    ("rd", 0, 1),
+    ("zr", 1, 1, 1),
+    ("zr", 1, 0, 3),
+    ("rd", 0, 2),
+    ("fx", 4),
+    ("zr", 1, 1, 2),
+    ("rf", 1, 1, 0),
+    ("rf", 1, 2, 0),
+    ("rf", 1, 2, 1),
+    ("rd", 0, 0),
+    ("sy", 0),
+    ("rd", 0, 3),
+    ("zr", 1, 1, 3),
+    ("rd", 1, 0),
+    ("rf", 1, 3, 1),
+    ("rf", 1, 3, 0),
+    ("fx", 1),
+    ("rd", 1, 1),
+    ("fx", 2),
+    ("rd", 1, 2),
+    ("sy", 4),
+    ("rd", 1, 3),
+    ("fx", 3),
+    ("sy", 1),
+    ("sy", 2),
+    ("sy", 3),
+)
+REDUCE_ORDER = (
+    ("pt", 0),
+    ("pt", 1),
+    ("op", 0),
+    ("g", 10),
+    ("pt", 2),
+    ("op", 1),
+    ("g", 6),
+    ("pt", 3),
+    ("rl", 1, 1),
+    ("rl", 1, 0),
+    ("rl", 0, 0),
+    ("rl", 0, 1),
+    ("op", 2),
+    ("g", 8),
+    ("to", 1),
+    ("rl", 2, 0),
+    ("rl", 3, 1),
+    ("rl", 4, 0),
+    ("rl", 3, 0),
+    ("g", 7),
+    ("rl", 2, 1),
+    ("rl", 4, 1),
+    ("op", 3),
+    ("to", 0),
+    ("rl", 5, 1),
+    ("mi", 1),
+    ("to", 2),
+    ("to", 3),
+    ("to", 4),
+    ("mi", 0),
+    ("rl", 5, 0),
+    ("rl", 6, 0),
+    ("rl", 6, 1),
+    ("lt", 1),
+    ("rl", 7, 1),
+    ("rl", 7, 0),
+    ("mi", 2),
+    ("mi", 3),
+    ("to", 5),
+    ("g", 0),
+    ("to", 6),
+    ("to", 7),
+    ("lt", 0),
+    ("mi", 4),
+    ("lt", 2),
+    ("g", 11),
+    ("gd", 0),
+    ("lt", 3),
+    ("mi", 5),
+    ("gd", 1),
+    ("pj", 0),
+    ("gd", 2),
+    ("g", 5),
+    ("lt", 4),
+    ("gd", 3),
+    ("mi", 6),
+    ("g", 3),
+    ("mi", 7),
+    ("pj", 1),
+    ("lt", 5),
+    ("gd", 4),
+    ("g", 1),
+    ("lt", 6),
+    ("gd", 5),
+    ("g", 4),
+    ("pj", 2),
+    ("lt", 7),
+    ("gd", 6),
+    ("g", 2),
+    ("gd", 7),
+    ("mb",),
+    ("pj", 3),
+    ("mb2",),
+    ("g", 9),
+    ("mb3",),
+    ("mf",),
+)
 
 
 def ring_place(index):
@@ -315,13 +456,17 @@
         self.slot = [o + upper * (RING - 1 - 2 * o) for o in order]
 
 
-def expert_kernel(
-    x_ref, cot_ref, small_ref, state_ref, gate_ref, up_ref, down_ref,
-    gate_out, up_out, down_out, mixed_out, small_out, state_out,
+def layer_kernel(
+    x_ref, cot_ref, small_ref, gate_ref, up_ref, down_ref, out_ref,
+    query_ref, key_ref, value_ref, logit_ref,
+    gate_out, up_out, down_out, proj_out, query_out, key_out, value_out, logit_out,
+    mixed, small_buf, small_out, state_buf, state_out, future_buf, future_out,
+    decayed, key_back, key_end, state_own, entry, span_end, scores, mixer_out, mixer_cot,
+    proj_to, proj_from, summed, terms, weights,
     x_all, cot_all, gate_pre, up_pre, hidden, gate_cot, up_cot,
     pair_to, pair_from, parts, first_in, second_in, total, half_total, z_in,
     tiny_send, tiny_recv, zs, zr, ps, pr, qs, qr,
-    bs, br, r1s, r1r, r2s, r2r, zts, ztr, ms, mr,
+    fs, fr, js, jr, bs, br, r1s, r1r, r2s, r2r, zts, ztr, ms, mr,
 ):
     here = Place()
     tok_rows, width = x_ref.shape
@@ -375,6 +520,7 @@
             )
         if part == 0:
             pair_send(a, slot, 0)
+            ring_send(a, (slot, 0))
         else:
             go(region, region, qs.at[a, slot, 4], qr.at[a, slot, 4], here.pair)
 
@@ -393,8 +539,6 @@
     def ring_send(a, unit):
         slot, part = unit
         n = number(unit)
-        for h, right_first in ((0, True), (1, False)):
-            pass
         for i, (h, device) in enumerate(
             ((0, here.right), (1, here.right), (0, here.left), (1, here.left))
         ):
@@ -406,14 +550,11 @@
         for copy in (right0, left1, right1, left0):
             copy.start()
 
-    def ring_forward(a, unit):
+    def ring_forward(a, unit, h):
         n = number(unit)
-        region = ring_region(a, unit, 3, 0)
-        arrived(pr.at[a, n, 0], region)
-        go(region, region, ps.at[a, n, 4], pr.at[a, n, 4], here.right)
-        region = ring_region(a, unit, 1, 1)
-        arrived(pr.at[a, n, 3], region)
-        go(region, region, ps.at[a, n, 5], pr.at[a, n, 5], here.left)
+        region = ring_region(a, unit, (3, 1)[h], h)
+        arrived(pr.at[a, n, 3 * h], region)
+        go(region, region, ps.at[a, n, 4 + h], pr.at[a, n, 4 + h], (here.right, here.left)[h])
 
     def ring_finish(a, unit):
         n = number(unit)
@@ -437,182 +578,285 @@
         source = own_rows(a, 0, lead) if slot == 0 and step == 0 else region
         go(source, region, qs.at[a, slot, step], qr.at[a, slot, step], here.pair)
 
-    def pair_wait(a, part):
+    def pair_wait(a, step):
         for slot in range(RING):
-            if part == 0:
-                for step in range(RING):
-                    arrived(qr.at[a, slot, step], pair_region(a, slot, step, 1 - here.core))
+            if step < 4:
+                arrived(qr.at[a, slot, step], pair_region(a, slot, step, 1 - here.core))
             else:
                 arrived(qr.at[a, slot, 4], piece(a, 1, slot, 1 - here.core))
 
-    for a in range(2):
-        z_start(a, 0)
-    ring_send(0, (0, 0))
-    for ref, out, i in ((small_ref, small_out, 0), (state_ref, state_out, 1)):
+    bf16, f32 = jnp.bfloat16, jnp.float32
+    key_cols = query_ref.shape[1]
+    heads = key_cols // DK
+    lane = lax.broadcasted_iota(jnp.int32, (1, key_cols), 1) // DK
+    row = lax.broadcasted_iota(jnp.int32, (key_cols, 1), 0) // DK
+
+    def dot(left, right, left_dim=1, right_dim=0, precision=None):
+        return lax.dot_general(
+            left, right, (((left_dim,), (right_dim,)), ((), ())),
+            precision=precision, preferred_element_type=f32,
+        )
+
+    def two(value):
+        high = value.astype(bf16)
+        return high, (value - high.astype(f32)).astype(bf16)
+
+    def triangle():
+        return lax.broadcasted_iota(jnp.int32, (tok_rows, tok_rows), 0) >= (
+            lax.broadcasted_iota(jnp.int32, (tok_rows, tok_rows), 1)
+        )
+
+    def only(value, h):
+        return jnp.where(lane == h, value, jnp.zeros_like(value))
+
+    def join(parts_of, which):
+        joined = parts_of[0]
+        for h in range(1, heads):
+            joined = jnp.where(which == h, parts_of[h], joined)
+        return joined
+
+    def head_cols(h):
+        return pl.ds(h * DV, DV)
+
+    def log_decay(logit):
+        return -(jnp.maximum(-logit, 0.0) + jnp.log(1.0 + jnp.exp(-jnp.abs(logit)))) / decay_temp
+
+    def column(s):
+        pick = (
+            lax.broadcasted_iota(jnp.int32, (small_buf.shape[0], DV), 0) == RING
+        ).astype(f32)
+        return dot(
+            small_out[s, :, pl.ds(0, key_cols)], pick, 0, 0, lax.Precision.HIGHEST
+        )
+
+    def mix_prepare():
+        ones = triangle().astype(bf16)
+        high, low = two(log_decay(logit_ref[...].astype(f32)))
+        cumulative = dot(ones, high) + dot(ones, low)
+        summed[...] = cumulative
+        last = cumulative[tok_rows - 1 : tok_rows, :]
+        keys = key_ref[...].astype(f32)
+        decayed[...] = (
+            query_ref[...].astype(f32) * DK ** (-0.5) * jnp.exp(cumulative)
+        ).astype(bf16)
+        key_back[...] = (keys * jnp.exp(-cumulative)).astype(bf16)
+        ends = (keys * jnp.exp(last - cumulative)).astype(bf16)
+        key_end[...] = ends
+        state = join([dot(ends, value_ref[:, head_cols(h)], 0, 0) for h in range(heads)], row)
+        state_own[...] = state
+        state_buf[...] = state.astype(bf16)
+        small_buf[:, pl.ds(0, tok_rows)] = small_ref[...]
+        small_buf[RING : RING + 1, pl.ds(0, key_cols)] = jnp.exp(last)
+        small_out[here.sp] = small_buf[...]
+        state_out[here.sp] = state_buf[...]
+        for i, (buf, out) in enumerate(((small_buf, small_out), (state_buf, state_out))):
+            for step, device in ((1, here.right), (3, here.left), (2, here.across)):
+                go(
+                    buf, out.at[here.sp], tiny_send.at[i, step - 1], tiny_recv.at[i, 3 - step],
+                    device,
+                )
+
+    def mix_forward():
+        for step in (1, 2, 3):
+            arrived(tiny_recv.at[0, step - 1], small_out.at[here.at[step]])
+            arrived(tiny_recv.at[1, step - 1], state_out.at[here.at[step]])
+        state = jnp.zeros((key_cols, DV), f32)
+        for s in range(RING - 1):
+            later = state * column(s) + state_out[s].astype(f32)
+            state = jnp.where(here.sp > s, later, state)
+        entry[...] = state.astype(bf16)
+        mine = (
+            lax.broadcasted_iota(jnp.int32, (small_buf.shape[0], 128), 0) == here.sp
+        ).astype(f32)
+        for s in range(RING):
+            weights[s] = dot(small_out[s], mine, 0, 0, lax.Precision.HIGHEST)[:tok_rows]
+        span_end[...] = state * column(here.sp) + state_own[...]
+        keep = triangle()
+        for h in range(heads):
+            mine = only(decayed[...], h)
+            score = jnp.where(keep, dot(mine, key_back[...], 1, 1), 0.0).astype(bf16)
+            scores[h] = score
+            mixer_out[:, head_cols(h)] = (
+                dot(score, value_ref[:, head_cols(h)]) + dot(mine, entry[...])
+            ).astype(bf16)
+
+    def mix_backward():
+        cot = [mixer_cot[:, head_cols(h)].astype(bf16) for h in range(heads)]
+        future = join([dot(decayed[...], cot[h], 0, 0) for h in range(heads)], row)
+        future_buf[...] = future.astype(bf16)
         for step, device in ((1, here.right), (3, here.left), (2, here.across)):
             go(
-                ref, out.at[here.sp], tiny_send.at[i, step - 1], tiny_recv.at[i, 3 - step], device
+                future_buf, future_out.at[here.sp], fs.at[step - 1], fr.at[3 - step], device
             )
-    ring_send(0, (0, 1))
-    ring_send(1, (0, 1))
+
+    held = {}
+
+    def mix_inner():
+        keep = triangle()
+        cot = [mixer_cot[:, head_cols(h)].astype(bf16) for h in range(heads)]
+        pairs = [
+            jnp.where(keep, dot(cot[h], value_ref[:, head_cols(h)], 1, 1), 0.0).astype(bf16)
+            for h in range(heads)
+        ]
+        inner = join(
+            [dot(cot[h], entry[...], 1, 1) + dot(pairs[h], key_back[...]) for h in range(heads)],
+            lane,
+        )
+        key_inner = join([dot(pairs[h], decayed[...], 0, 0) for h in range(heads)], lane)
+        query_out[...] = jnp.exp(summed[...]) * inner * DK ** (-0.5)
+        key_out[...] = jnp.exp(-summed[...]) * key_inner
+        terms[...] = (
+            decayed[...].astype(f32) * inner - key_back[...].astype(f32) * key_inner
+        )
+        for h in range(heads):
+            value_out[:, head_cols(h)] = dot(scores[h], cot[h], 0, 0)
+
+    def mix_outer():
+        for step in (1, 2, 3):
+            arrived(fr.at[step - 1], future_out.at[here.at[step]])
+        state = jnp.zeros((key_cols, DV), f32)
+        for s in range(RING - 1, 0, -1):
+            earlier = state * column(s) + future_out[s].astype(f32)
+            state = jnp.where(here.sp < s, earlier, state)
+        ahead = state.astype(bf16)
+        key_outer = join(
+            [dot(value_ref[:, head_cols(h)], ahead, 1, 1) for h in range(heads)], lane
+        )
+        last = summed[tok_rows - 1 : tok_rows, :]
+        key_out[...] += jnp.exp(last - summed[...]) * key_outer
+        for h in range(heads):
+            value_out[:, head_cols(h)] += dot(only(key_end[...], h), ahead)
+        high, low = two(terms[...] - key_end[...].astype(f32) * key_outer)
+        ones = triangle().astype(bf16)
+        tail_sum = dot(ones, high, 0, 0) + dot(ones, low, 0, 0)
+        beyond = dot(
+            jnp.ones((8, DV), f32), state * span_end[...], 1, 1, lax.Precision.HIGHEST
+        )[0:1, :]
+        logit_out[...] = (tail_sum + beyond) / (
+            decay_temp * (1.0 + jnp.exp(logit_ref[...].astype(f32)))
+        )
+
+    def mix_finish():
+        for m in range(RING):
+            result = proj_to[m, here.sp].astype(f32)
+            for step in (1, 3, 2):
+                arrived(jr.at[m, step - 1], proj_from.at[m, here.at[step]])
+                result = result + proj_from[m, here.at[step]].astype(f32)
+            proj_out[pl.ds(m * atom, atom), :] = result
+
+    def block_of(ref, s):
+        if s is None:
+            return ref[:, pl.ds(lead, tail), :].reshape(RING * tail, ref.shape[2])
+        return ref[s, pl.ds(0, lead), :]
+
+    def keep_block(ref, s, value):
+        if s is None:
+            ref[:, pl.ds(lead, tail), :] = value.reshape(RING, tail, ref.shape[2])
+        else:
+            ref[s, pl.ds(0, lead), :] = value
+
+    def forward_rows(s):
+        block = block_of(x_all, s)
+        keep_block(gate_pre, s, contract_cols(block, gate_ref[...]))
+        keep_block(up_pre, s, contract_cols(block, up_ref[...]))
+
+    def second_rows(s):
+        weight = jnp.concatenate([block_of(weights, s)] * (width // 128), axis=1)
+        hidden_cot = contract_cols(block_of(cot_all, s), down_ref[...]) * weight
+        gp, upp = block_of(gate_pre, s), block_of(up_pre, s)
+        sig = 1.0 / (1.0 + jnp.exp(-gp))
+        active = gp * sig
+        keep_block(hidden, s, (active * upp * weight).astype(jnp.bfloat16))
+        keep_block(up_cot, s, (hidden_cot * active).astype(jnp.bfloat16))
+        keep_block(
+            gate_cot, s,
+            (hidden_cot * upp * sig * (1.0 + gp * (1.0 - sig))).astype(jnp.bfloat16),
+        )
+
+    def rows_of(a, step, work):
+        pair_wait(a, step)
+        work(here.at[step] if step < RING else None)
+
+    def own_start(a):
+        ring_send(a, (0, 0))
+        pair_send(a, 0, 0)
+
+    gather_steps = {
+        "zs": z_start,
+        "rs": lambda a, n: own_start(a) if n == 0 else ring_send(a, (0, 1)),
+        "zr": z_relay,
+        "rf": lambda a, n, h: ring_forward(a, (n % 4, n // 4), h),
+        "rd": lambda a, n: ring_finish(a, (n % 4, n // 4)),
+        "prep": mix_prepare,
+        "mixf": mix_forward,
+        "fx": lambda i: rows_of(0, i, forward_rows),
+        "sy": lambda i: rows_of(1, i, second_rows),
+    }
     for a in range(2):
         alls[a][here.sp, :, cols(0, here.core)] = ins[a][...]
-        pair_send(a, 0, 0)
-    small_out[here.sp] = small_ref[...]
-    state_out[here.sp] = state_ref[...]
-    z_relay(0, 0, 1)
-    ring_send(0, (1, 0))
-    ring_forward(0, (0, 0))
-    ring_forward(0, (0, 1))
-    ring_forward(1, (0, 1))
-    z_relay(0, 0, 2)
-    ring_send(0, (2, 0))
-    ring_forward(0, (1, 0))
-    ring_finish(0, (0, 0))
-    z_relay(0, 0, 3)
-    ring_send(0, (3, 0))
-    ring_forward(0, (2, 0))
-    ring_finish(0, (1, 0))
-    z_relay(1, 0, 1)
-    ring_send(1, (0, 0))
-    ring_send(1, (1, 0))
-    ring_forward(0, (3, 0))
-    ring_finish(0, (2, 0))
-    z_relay(1, 0, 2)
-    ring_send(1, (2, 0))
-    ring_finish(0, (0, 1))
-    z_relay(1, 0, 3)
-    ring_send(1, (3, 0))
-    ring_finish(1, (0, 1))
-    ring_forward(1, (0, 0))
-    ring_finish(0, (3, 0))
-    pair_wait(0, 0)
-
-    def forward_rows(s, start, count):
-        rows = pl.ds(start, count)
-        block = x_all[s, rows, :]
-        gate_pre[s, rows, :] = contract_cols(block, gate_ref[...])
-        up_pre[s, rows, :] = contract_cols(block, up_ref[...])
-
-    half = lead // 2
-    steps = [
-        lambda: ring_forward(1, (1, 0)),
-        lambda: z_relay(0, 1, 1),
-        lambda: ring_finish(1, (0, 0)),
-        lambda: z_relay(0, 1, 2),
-        lambda: ring_forward(1, (2, 0)),
-        lambda: ring_finish(1, (1, 0)),
-        lambda: z_relay(0, 1, 3),
-        lambda: ring_forward(1, (3, 0)),
-    ]
-    for i in range(8):
-        forward_rows(i // 2, (i % 2) * half, half)
-        steps[i]()
-    for s in range(RING):
-        for step in (1, 2, 3):
-            pass
-    for step in (1, 2, 3):
-        arrived(tiny_recv.at[0, step - 1], small_out.at[here.at[step]])
-        arrived(tiny_recv.at[1, step - 1], state_out.at[here.at[step]])
-    ring_finish(1, (2, 0))
-    z_relay(1, 1, 1)
-    pair_wait(0, 1)
-    for s in range(RING):
-        forward_rows(s, lead, tail)
-    z_relay(1, 1, 2)
-    z_relay(1, 1, 3)
-    ring_finish(1, (3, 0))
-    pair_wait(1, 0)
-
-    pick = (
-        lax.broadcasted_iota(jnp.int32, (small_ref.shape[0], 128), 0) == here.sp
-    ).astype(jnp.float32)
-
-    def second_rows(s, start, count):
-        rows = pl.ds(start, count)
-        weight = lax.dot_general(
-            small_out[s, :, pl.ds(0, tok_rows)][:, start : start + count],
-            pick,
-            (((0,), (0,)), ((), ())),
-            precision=lax.Precision.HIGHEST,
-            preferred_element_type=jnp.float32,
-        )
-        weight = jnp.concatenate([weight] * (width // 128), axis=1)
-        hidden_cot = contract_cols(cot_all[s, rows, :], down_ref[...]) * weight
-        gp, upp = gate_pre[s, rows, :], up_pre[s, rows, :]
-        sig = 1.0 / (1.0 + jnp.exp(-gp))
-        active = gp * sig
-        hidden[s, rows, :] = (active * upp * weight).astype(jnp.bfloat16)
-        up_cot[s, rows, :] = (hidden_cot * active).astype(jnp.bfloat16)
-        gate_cot[s, rows, :] = (hidden_cot * upp * sig * (1.0 + gp * (1.0 - sig))).astype(
-            jnp.bfloat16
-        )
-
-    for i in range(8):
-        second_rows(i // 2, (i % 2) * half, half)
-    pair_wait(1, 1)
-    for s in range(RING):
-        second_rows(s, lead, tail)
+    for name, *rest in GATHER_ORDER:
+        gather_steps[name](*rest)
 
     pieces, wide = parts.shape[0], parts.shape[3]
     split = tok_rows // 2
-    per = width // wide
-
-    def back_cols(k, core):
-        at = (2 * (k // per) + core) * width + (k % per) * wide
-        return pl.ds(pl.multiple_of(at, wide), wide)
-
-    def partial(k, step, core):
-        c = back_cols(k, core)
-        s = here.at[step]
-        return jnp.dot(
-            gate_cot[s], gate_ref[:, c], preferred_element_type=jnp.float32
-        ) + jnp.dot(up_cot[s], up_ref[:, c], preferred_element_type=jnp.float32)
-
-    ring_order = (2, 1, 3, 0)
-
-    def pair_part(k):
-        for step in ring_order:
-            pair_to[k, step] = partial(k, step, 1 - here.core).astype(jnp.bfloat16)
+    span = gate_ref.shape[1] // RING
+    atom = span // RING
+    per = 2 * atom // wide
+
+    def atoms(k, core):
+        for i in range(wide // atom):
+            target = 2 * core + (k % per) + i
+            yield pl.ds(pl.multiple_of(target * span + (k // per) * atom, atom), atom)
+
+    def columns(ref, k, core):
+        return jnp.concatenate([ref[:, c] for c in atoms(k, core)], axis=1)
+
+    top, bottom = pl.ds(0, split), pl.ds(split, split)
+
+    def partial(m, core):
+        rows = RING * tok_rows
+        total_of = [
+            jnp.dot(
+                cot[...].reshape(rows, width),
+                jnp.concatenate([columns(ref, m * per + i, core) for i in range(per)], axis=1),
+                preferred_element_type=jnp.float32,
+            )
+            for cot, ref in ((gate_cot, gate_ref), (up_cot, up_ref))
+        ]
+        both = total_of[0] + total_of[1]
+        for i in range(per):
+            part = both[:, i * wide : (i + 1) * wide]
+            yield m * per + i, part.reshape(RING, tok_rows, wide)
+
+    def pair_part(m):
+        for k, part in partial(m, 1 - here.core):
+            pair_to[k] = part.astype(jnp.bfloat16)
+            go(pair_to.at[k], pair_from.at[k], bs.at[k], br.at[k], here.pair)
+
+    def own_part(m):
+        for k, part in partial(m, here.core):
+            arrived(br.at[k], pair_from.at[k])
+            parts[k] = (part + pair_from[k].astype(jnp.float32)).astype(jnp.bfloat16)
+            right, across, left = [parts.at[k, here.at[i]] for i in (1, 2, 3)]
+            go(across.at[top], first_in.at[k, 0], r1s.at[k, 0], r1r.at[k, 0], here.right)
+            go(across.at[bottom], first_in.at[k, 1], r1s.at[k, 1], r1r.at[k, 1], here.left)
             go(
-                pair_to.at[k, step], pair_from.at[k, step], bs.at[k, step], br.at[k, step], here.pair
+                right.at[bottom], second_in.at[k, 0, bottom], r2s.at[k, 0], r2r.at[k, 0],
+                here.right,
             )
-
-    top, bottom = pl.ds(0, split), pl.ds(split, split)
-
-    def own_part(k):
-        for step in ring_order:
-            mine = partial(k, step, here.core)
-            arrived(br.at[k, step], pair_from.at[k, step])
-            parts[k, step] = (mine + pair_from[k, step].astype(jnp.float32)).astype(jnp.bfloat16)
-            if step == 2:
-                go(parts.at[k, 2, top], first_in.at[k, 0], r1s.at[k, 0], r1r.at[k, 0], here.right)
-                go(parts.at[k, 2, bottom], first_in.at[k, 1], r1s.at[k, 1], r1r.at[k, 1], here.left)
-            if step == 1:
-                go(
-                    parts.at[k, 1, bottom], second_in.at[k, 0, bottom],
-                    r2s.at[k, 0], r2r.at[k, 0], here.right,
-                )
-            if step == 3:
-                go(
-                    parts.at[k, 3, top], second_in.at[k, 1, top],
-                    r2s.at[k, 1], r2r.at[k, 1], here.left,
-                )
+            go(left.at[top], second_in.at[k, 1, top], r2s.at[k, 1], r2r.at[k, 1], here.left)
 
     def add_to(ref, other):
         ref[...] = (ref[...].astype(jnp.float32) + other.astype(jnp.float32)).astype(jnp.bfloat16)
 
-    def ring_relay(k):
-        arrived(r1r.at[k, 0], first_in.at[k, 0])
-        add_to(parts.at[k, 1, top], first_in[k, 0])
+    def ring_relay(k, h):
+        step, rows, device = ((1, top, here.right), (3, bottom, here.left))[h]
+        arrived(r1r.at[k, h], first_in.at[k, h])
+        mine = parts.at[k, here.at[step]].at[rows]
+        add_to(mine, first_in[k, h])
         go(
-            parts.at[k, 1, top], second_in.at[k, 0, top], r2s.at[k, 2], r2r.at[k, 2], here.right
-        )
-        arrived(r1r.at[k, 1], first_in.at[k, 1])
-        add_to(parts.at[k, 3, bottom], first_in[k, 1])
-        go(
-            parts.at[k, 3, bottom], second_in.at[k, 1, bottom],
-            r2s.at[k, 3], r2r.at[k, 3], here.left,
+            mine, second_in.at[k, h, rows],
+            r2s.at[k, 2 + h], r2r.at[k, 2 + h], device,
         )
 
     def ring_total(k):
@@ -621,7 +865,7 @@
         arrived(r2r.at[k, 2], second_in.at[k, 0, top])
         arrived(r2r.at[k, 3], second_in.at[k, 1, bottom])
         total[k] = (
-            parts[k, 0].astype(jnp.float32)
+            parts[k, here.sp].astype(jnp.float32)
             + second_in[k, 0].astype(jnp.float32)
             + second_in[k, 1].astype(jnp.float32)
         ).astype(jnp.bfloat16)
@@ -641,15 +885,14 @@
         guarded.append((here.inner, copy))
 
     def line_total(k):
-        c = back_cols(k, here.core)
-        region = mixed_out.at[:, c]
+        region = mixed.at[k, here.core]
         copy = remote(region, region, ms.at[k, 0], mr.at[k, 0], here.near)
 
         @pl.when(here.inner)
         def _():
             arrived(ztr.at[k, 1], z_in.at[k, 1])
-            mixed_out[:, c] = (
-                cot_all[here.sp, :, c].astype(jnp.float32)
+            mixed[k, here.core] = (
+                columns(cot_all.at[here.sp], k, here.core).astype(jnp.float32)
                 + (half_total[k].astype(jnp.float32) + z_in[k, 1].astype(jnp.float32))
             ).astype(jnp.bfloat16)
             copy.start()
@@ -663,44 +906,64 @@
         go(region, region, ms.at[k, 1], mr.at[k, 1], here.pair)
 
     features = gate_ref.shape[1]
-    blocks = features // width
+    block_cols = 2 * width
 
     def weight_grad(n):
-        which, j = n // blocks, n % blocks
+        which, j = n % 3, n // 3
         left, right, out = (
             (gate_cot, x_all, gate_out), (up_cot, x_all, up_out), (hidden, cot_all, down_out)
         )[which]
-        c = pl.ds(j * width, width)
+        c = pl.ds(j * block_cols, block_cols)
         rows = RING * tok_rows
         out[:, c] = contract_rows(
-            left[...].reshape(rows, width), right[:, :, c].reshape(rows, width)
-        )
-
-    grads = list(range(3 * blocks))
-
-    def some_grads(count):
-        for _ in range(min(count, len(grads))):
-            weight_grad(grads.pop(0))
-
-    lanes = []
-    pair_part(0)
-    for k in range(pieces + 5):
-        if k + 1 < pieces:
-            pair_part(k + 1)
-        if k < pieces:
-            own_part(k)
-        some_grads(-(-3 * blocks // (pieces + 4)))
-        if 0 <= k - 1 < pieces:
-            ring_relay(k - 1)
-        if 0 <= k - 2 < pieces:
-            ring_total(k - 2)
-        if 0 <= k - 3 < pieces:
-            line_middle(k - 3)
-        if 0 <= k - 4 < pieces:
-            line_total(k - 4)
-    some_grads(3 * blocks)
-    for k in range(pieces):
-        arrived(mr.at[k, 1], mixed_out.at[:, back_cols(k, 1 - here.core)])
+            left[...].reshape(rows, width), right[:, :, c].reshape(rows, block_cols)
+        )
+
+    def mixed_group(m):
+        return jnp.concatenate(
+            [mixed[m * per + i, core] for core in range(2) for i in range(per)], axis=1
+        )
+
+    def group_done(k):
+        arrived(mr.at[k, 1], mixed.at[k, 1 - here.core])
+        if (k + 1) % per:
+            return
+        m = k // per
+        group = mixed_group(m)
+        weight = jnp.concatenate(
+            [out_ref[pl.ds(d * span + m * atom, atom), :] for d in range(RING)], axis=0
+        )
+        term = dot(group, weight)
+        mixer_cot[...] = term if m == 0 else mixer_cot[...] + term
+
+    def group_proj(m):
+        group = mixed_group(m)
+        block = dot(group, mixer_out[...], 0, 0).astype(bf16)
+        for d in range(RING):
+            proj_to[m, d] = block[d * atom : (d + 1) * atom, :]
+        for step, device in ((1, here.right), (3, here.left), (2, here.across)):
+            go(
+                proj_to.at[m, here.at[step]], proj_from.at[m, here.sp],
+                js.at[m, step - 1], jr.at[m, 3 - step], device,
+            )
+
+    reduce_steps = {
+        "pt": pair_part,
+        "op": own_part,
+        "g": weight_grad,
+        "rl": ring_relay,
+        "to": ring_total,
+        "mi": line_middle,
+        "lt": line_total,
+        "gd": group_done,
+        "pj": group_proj,
+        "mb": mix_backward,
+        "mb2": mix_inner,
+        "mb3": mix_outer,
+        "mf": mix_finish,
+    }
+    for name, *rest in REDUCE_ORDER:
+        reduce_steps[name](*rest)
     for copy in plain:
         copy.wait_send()
     for cond, copy in guarded:
@@ -709,26 +972,43 @@
             copy.wait_send()
 
 
-def expert_stage(x, cot, small, state, gate, up, down):
+def layer_stage(x, cot, small, gate, up, down, out_weight, query, key_in, value, logit):
     tok_rows, width = x.shape
     hidden_dev, features = gate.shape
-    pieces, wide = 4, 2 * features // (2 * RING * 2)
+    key_cols, value_cols = query.shape[1], value.shape[1]
+    heads = key_cols // DK
+    pieces = PIECES
+    wide = features // (2 * pieces)
     vmem = pl.BlockSpec(memory_space=pltpu.VMEM)
     dma = pltpu.SemaphoreType.DMA
     f32, bf16 = jnp.float32, jnp.bfloat16
     full = (RING, tok_rows, features)
     acts = (RING, tok_rows, hidden_dev)
     block = (tok_rows, wide)
+    state = (key_cols, DV)
+    proj = (RING, RING, features // RING**2, value_cols)
+    table = (small.shape[0], -(-max(tok_rows, key_cols) // 128) * 128)
+    results = [(hidden_dev, features)] * 3 + [
+        (features // RING, value_cols), query.shape, key_in.shape, value.shape, logit.shape
+    ]
     return pl.pallas_call(
-        expert_kernel,
-        out_shape=[jax.ShapeDtypeStruct((hidden_dev, features), f32)] * 3 + [
-            jax.ShapeDtypeStruct((tok_rows, features), bf16),
-            jax.ShapeDtypeStruct((RING,) + small.shape, small.dtype),
-            jax.ShapeDtypeStruct((RING,) + state.shape, state.dtype),
-        ],
-        in_specs=[vmem] * 7,
-        out_specs=[vmem] * 6,
+        layer_kernel,
+        out_shape=[jax.ShapeDtypeStruct(shape, f32) for shape in results],
+        in_specs=[vmem] * 11,
+        out_specs=[vmem] * 8,
         scratch_shapes=[
+            pltpu.VMEM((pieces, 2) + block, bf16),
+            pltpu.VMEM(table, f32), pltpu.VMEM((RING,) + table, f32),
+            pltpu.VMEM(state, bf16), pltpu.VMEM((RING,) + state, bf16),
+            pltpu.VMEM(state, bf16), pltpu.VMEM((RING,) + state, bf16),
+            pltpu.VMEM(query.shape, bf16), pltpu.VMEM(query.shape, bf16),
+            pltpu.VMEM(query.shape, bf16),
+            pltpu.VMEM(state, f32), pltpu.VMEM(state, bf16), pltpu.VMEM(state, f32),
+            pltpu.VMEM((heads, tok_rows, tok_rows), bf16),
+            pltpu.VMEM(value.shape, bf16), pltpu.VMEM(value.shape, f32),
+            pltpu.VMEM(proj, bf16), pltpu.VMEM(proj, bf16),
+            pltpu.VMEM(query.shape, f32), pltpu.VMEM(query.shape, f32),
+            pltpu.VMEM((RING, tok_rows, 128), f32),
             pltpu.VMEM(full, bf16), pltpu.VMEM(full, bf16),
             pltpu.VMEM(acts, f32), pltpu.VMEM(acts, f32),
             pltpu.VMEM(acts, bf16), pltpu.VMEM(acts, bf16), pltpu.VMEM(acts, bf16),
@@ -742,7 +1022,8 @@
             dma((2, 2, 5)), dma((2, 2, 3)),
             dma((2, 5, 6)), dma((2, 5, 6)),
             dma((2, 4, 5)), dma((2, 4, 5)),
-            dma((pieces, 4)), dma((pieces, 4)),
+            dma((3,)), dma((3,)), dma((RING, 3)), dma((RING, 3)),
+            dma((pieces,)), dma((pieces,)),
             dma((pieces, 2)), dma((pieces, 2)),
             dma((pieces, 4)), dma((pieces, 4)),
             dma((pieces, 2)), dma((pieces, 2)),
@@ -751,134 +1032,50 @@
         compiler_params=pltpu.CompilerParams(
             collective_id=0, has_side_effects=True, vmem_limit_bytes=60 << 20
         ),
-        name="expert_stage",
-    )(x, cot, small, state, gate, up, down)
-
-
-def exchange_kernel(x_ref, out_ref, send_sem, recv_sem):
-    here = Place()
-    devices = (here.right, here.across, here.left)
-    greet(devices)
-    sends = []
-    for step in (1, 3, 2):
-        copy = remote(
-            x_ref.at[here.at[step]], out_ref.at[here.sp],
-            send_sem.at[step - 1], recv_sem.at[3 - step], devices[step - 1],
-        )
+        name="layer_stage",
+    )(x, cot, small, gate, up, down, out_weight, query, key_in, value, logit)
+
+
+def write_kernel(*refs):
+    count = len(refs) // 2
+    sems = refs[-1]
+    copies = [
+        pltpu.make_async_copy(refs[i], refs[count + i], sems.at[i]) for i in range(count)
+    ]
+    for copy in copies:
         copy.start()
-        sends.append(copy)
-    out_ref[here.sp] = x_ref[here.sp]
-    for step in (1, 2, 3):
-        arrived(recv_sem.at[step - 1], out_ref.at[here.at[step]])
-    for copy in sends:
-        copy.wait_send()
-
-
-def exchange(x, number):
-    vmem = pl.BlockSpec(memory_space=pltpu.VMEM)
-    dma = pltpu.SemaphoreType.DMA
+    for copy in copies:
+        copy.wait()
+
+
+def write_out(arrays):
     return pl.pallas_call(
-        exchange_kernel,
-        out_shape=jax.ShapeDtypeStruct(x.shape, x.dtype),
-        in_specs=[vmem],
-        out_specs=vmem,
-        scratch_shapes=[dma((3,)), dma((3,))],
-        compiler_params=pltpu.CompilerParams(collective_id=number, has_side_effects=True),
-        name="exchange" + str(number),
-    )(x)
+        write_kernel,
+        out_shape=[jax.ShapeDtypeStruct(a.shape, a.dtype) for a in arrays],
+        in_specs=[pl.BlockSpec(memory_space=pltpu.VMEM)] * len(arrays),
+        out_specs=[pl.BlockSpec(memory_space=pltpu.HBM)] * len(arrays),
+        scratch_shapes=[pltpu.SemaphoreType.DMA((len(arrays),))],
+        name="write_out",
+    )(*arrays)
 
 
 def ring_local(
     layer_in, out_cot, route_ids, route_probs, group_prob, gate_weight, up_weight,
     down_weight, out_weight, query, key_in, value, decay_logit,
 ):
-    tok_rows, local_cols = layer_in.shape
-    experts_all = lax.axis_size("sp")
-    here = lax.axis_index("sp")
-    route_weight = group_prob[:, None] * route_probs / jnp.sum(route_probs, axis=1, keepdims=True)
-    table = jnp.sum(
+    total = route_probs[:, 0] + route_probs[:, 1]
+    expert = jnp.arange(8, dtype=jnp.int32)[:, None]
+    small = sum(
         jnp.where(
-            route_ids[None] == jnp.arange(experts_all, dtype=jnp.int32)[:, None, None],
-            route_weight[None],
-            0.0,
-        ),
-        axis=2,
-    )
-    head_dev = query.shape[1] // DK
-
-    def heads(tensor):
-        return tensor.astype(jnp.float32).reshape(tok_rows, head_dev, -1).transpose(1, 0, 2)
-
-    def flat(tensor):
-        return tensor.transpose(1, 0, 2).reshape(tok_rows, -1)
-
-    def product(spec, a, b):
-        return jnp.einsum(spec, a, b, precision=highest)
-
-    scaled_query = heads(query) * DK ** (-0.5)
-    key_h, value_h, logit_h = heads(key_in), heads(value), heads(decay_logit)
-    causal = jnp.tril(jnp.ones((tok_rows, tok_rows), dtype=bool))
-    ones = causal.astype(jnp.float32)
-    cumulative = product("cs,hsd->hcd", ones, jax.nn.log_sigmoid(logit_h) / decay_temp)
-    span_log = cumulative[:, -1:, :]
-    growth, shrink = jnp.exp(cumulative), jnp.exp(-cumulative)
-    to_end = jnp.exp(span_log - cumulative)
-    query_decayed, key_back, key_to_end = scaled_query * growth, key_h * shrink, key_h * to_end
-    span_decay = jnp.exp(span_log[:, 0, :])
-    span_state = product("hcd,hcv->hdv", key_to_end, value_h)
-    lanes = -(-max(tok_rows, head_dev * DK) // 128) * 128
-    small = jnp.zeros((8, lanes), jnp.float32)
-    small = small.at[:experts_all, :tok_rows].set(table)
-    small = small.at[experts_all, : head_dev * DK].set(span_decay.reshape(-1))
-    gate_g, up_g, down_g, full_mixed, smalls, states = expert_stage(
-        layer_in, out_cot, small, span_state.astype(jnp.bfloat16).reshape(head_dev * DK, DV),
-        gate_weight[0], up_weight[0], down_weight[0],
-    )
-    decays = smalls[:, experts_all, : head_dev * DK].reshape(RING, head_dev, DK, 1)
-    states = states.astype(jnp.float32).reshape(RING, head_dev, DK, DV)
-    entry_state = jnp.zeros((head_dev, DK, DV), jnp.float32)
-    for s in range(RING - 1):
-        entry_state = jnp.where(s < here, entry_state * decays[s] + states[s], entry_state)
-    span_end = span_decay[..., None] * entry_state + span_state
-    scores = jnp.where(causal, product("hcd,hsd->hcs", query_decayed, key_back), 0.0)
-    outputs = product("hcs,hsv->hcv", scores, value_h) + product(
-        "hcd,hdv->hcv", query_decayed, entry_state
-    )
-    mixer_out = flat(outputs).astype(jnp.bfloat16)
-    mixer_cot = jnp.dot(full_mixed, out_weight, preferred_element_type=jnp.float32)
-    proj_parts = contract_rows(full_mixed, mixer_out).astype(jnp.bfloat16)
-    proj_parts = exchange(proj_parts.reshape(RING, -1, proj_parts.shape[1]), 1)
-    proj_grad = jnp.sum(proj_parts.astype(jnp.float32), axis=0)
-    cot_h = heads(mixer_cot)
-    span_future = product("hcd,hcv->hdv", query_decayed, cot_h)
-    futures = exchange(
-        jnp.broadcast_to(
-            span_future.astype(jnp.bfloat16).reshape(1, head_dev * DK, DV), (RING, head_dev * DK, DV)
-        ),
-        2,
-    )
-    futures = futures.astype(jnp.float32).reshape(RING, head_dev, DK, DV)
-    future_state = jnp.zeros((head_dev, DK, DV), jnp.float32)
-    for s in range(RING - 1, 0, -1):
-        future_state = jnp.where(s > here, future_state * decays[s] + futures[s], future_state)
-    cot_values = jnp.where(causal, product("hcv,hsv->hcs", cot_h, value_h), 0.0)
-    query_scaled_grad = growth * (
-        product("hcv,hdv->hcd", cot_h, entry_state) + product("hcs,hsd->hcd", cot_values, key_back)
-    )
-    key_grad = shrink * product("hcs,hcd->hsd", cot_values, query_decayed) + to_end * product(
-        "hsv,hdv->hsd", value_h, future_state
-    )
-    value_grad = product("hcs,hcv->hsv", scores, cot_h) + product(
-        "hsd,hdv->hsv", key_to_end, future_state
-    )
-    decay_terms = scaled_query * query_scaled_grad - key_h * key_grad
-    tail_sum = product("cs,hcd->hsd", ones, decay_terms)
-    log_grad = tail_sum + jnp.sum(future_state * span_end, axis=2)[:, None, :]
-    logit_grad = flat(log_grad * jax.nn.sigmoid(-logit_h) / decay_temp)
-    return (
-        gate_g[None], up_g[None], down_g[None], proj_grad,
-        flat(query_scaled_grad * DK ** (-0.5)), flat(key_grad), flat(value_grad), logit_grad,
-    )
+            route_ids[:, j][None] == expert, (group_prob * route_probs[:, j] / total)[None], 0.0
+        )
+        for j in range(2)
+    )
+    results = write_out(layer_stage(
+        layer_in, out_cot, small, gate_weight[0], up_weight[0], down_weight[0],
+        out_weight, query, key_in, value, decay_logit,
+    ))
+    return tuple(r[None] for r in results[:3]) + tuple(results[3:])
 
 
 def solution(mesh):

time: 172 us -> 117 us (0.68)
  Pallas kernels: 139 us -> 113 us
  local copies, waits for them, and re-layouts: 15.6 us -> 1.56 us
  matrix products: 12 us -> 0 us
  other arithmetic: 3.53 us -> 1.3 us
    pallas_call x3 -> x2, Pallas kernels: 139 us -> 113 us  [the longest x1 107 us: layer_stage(): pl.pallas_call(layer_kernel, out_shape=[jax.ShapeDtypeStruct(shape, f32)...]
    dot_general x15 -> x0, matrix products: 11.8 us -> none  [the longest x13 8.19 us: product(): return jnp.einsum(spec, a, b, precision=highest)]
    unnamed x35 -> x0, local copies, waits for them, and re-layouts: 11.5 us -> none
    reduce_sum x4 -> x0, other arithmetic: 2.48 us -> none  [the longest x1 2.21 us: ring_local(): proj_grad = jnp.sum(proj_parts.astype(jnp.float32), axis=0)]
where the time goes in v2:
time: 117 us
  Pallas kernels  113 us (97%)
  local copies, waits for them, and re-layouts  1.56 us (1%)
  other arithmetic  1.3 us (1%)
    pallas_call x1, Pallas kernels, layer_stage(): pl.pallas_call(layer_kernel, out_shape=[jax.ShapeDtypeStruct(shape, f32)...  107 us
    pallas_call x1, Pallas kernels, write_out(): pl.pallas_call(write_kernel, out_shape=[jax.ShapeDtypeStruct(a.shape, a.d...  6.23 us

profile of v2, /device:TPU:0, one launch (start us, length us, event | category | flops | bytes accessed | tf_op | source)
XLA Modules:
  0.0 116.6 jit_solution(10809115976941118469)
XLA Ops:
  0.6 0.8 slice_reduce_fusion.3
  1.4 0.8 slice_reduce_fusion.2
  2.2 0.7 multiply_divide_fusion.1
  2.9 0.6 select_add_fusion.small_ref
  3.5 106.7 %layer_stage.1 = (f32[256,2048]{1,0:T(8,128)}, f32[256,2048]{1,0:T(8,128)}, f32[256,2048]{1,0:T(8,128)}, f32[512,256]{1,0:T(8,128)}, f32[320,128]{1,0:T(8,128)},...) custom-call(bf16[320,256]{1,0:T(8,128)(2,1)} %x_ref.1, bf16[320,256]{1,0:T(8,128)(2,1)} %cot_ref.1, ...), custom_call_target="tpu_custom_call" | custom-call | tf_op jit(solution)/shard_map/layer_stage/pallas_call | solution.py:994
  110.2 6.2 %write_out.1 = (f32[256,2048]{1,0:T(8,128)}, f32[256,2048]{1,0:T(8,128)}, f32[256,2048]{1,0:T(8,128)}, f32[512,256]{1,0:T(8,128)}, f32[320,128]{1,0:T(8,128)}, /...) custom-call(f32[256,2048]{1,0:T(8,128)} %get-tuple-element.24.refs_0_, ...), custom_call_target="tpu_custom_call" | custom-call | tf_op jit(solution)/shard_map/write_out/pallas_call | solution.py:1052

commit v3 on v2

--- a/solution.py
+++ b/solution.py
@@ -269,142 +269,176 @@
 EXPERT_CUT = 5
 PIECES = 8
 GATHER_ORDER = (
+    ("zs", 0, 0),
     ("rs", 1, 4),
     ("rs", 0, 4),
-    ("zs", 0, 0),
     ("zs", 1, 0),
     ("rs", 0, 0),
     ("rf", 0, 4, 1),
+    ("rf", 1, 4, 1),
+    ("prep",),
+    ("rf", 1, 4, 0),
     ("rf", 0, 4, 0),
-    ("prep",),
-    ("rf", 1, 4, 1),
-    ("rf", 1, 4, 0),
+    ("rn", 0, 4),
     ("zr", 0, 0, 1),
+    ("rf", 0, 0, 1),
     ("rs", 1, 0),
+    ("rn", 1, 4),
     ("zr", 0, 0, 2),
     ("zr", 1, 0, 1),
-    ("rd", 0, 4),
+    ("ro", 1, 4),
+    ("ro", 0, 4),
+    ("rf", 0, 1, 0),
     ("zr", 0, 0, 3),
+    ("rf", 0, 1, 1),
+    ("zr", 1, 1, 1),
+    ("zr", 1, 0, 2),
+    ("rf", 1, 0, 1),
+    ("zr", 0, 1, 2),
+    ("rn", 0, 1),
+    ("rf", 1, 1, 0),
+    ("rf", 0, 0, 0),
+    ("rf", 0, 2, 0),
     ("mixf",),
-    ("rd", 1, 4),
-    ("rf", 0, 1, 1),
+    ("rf", 1, 1, 1),
+    ("rf", 0, 2, 1),
+    ("rn", 0, 0),
+    ("rn", 1, 1),
+    ("zr", 1, 1, 3),
     ("fx", 0),
-    ("rf", 0, 1, 0),
-    ("rf", 0, 0, 1),
-    ("zr", 0, 1, 2),
-    ("rf", 0, 2, 1),
-    ("rf", 0, 0, 0),
     ("zr", 0, 1, 1),
-    ("rf", 0, 2, 0),
-    ("zr", 1, 0, 2),
+    ("rf", 1, 0, 0),
+    ("rn", 1, 0),
     ("rf", 0, 3, 1),
     ("rf", 0, 3, 0),
+    ("rn", 0, 2),
+    ("rn", 0, 3),
+    ("zr", 1, 0, 3),
+    ("fx", 1),
+    ("rf", 1, 2, 1),
+    ("rf", 1, 2, 0),
     ("zr", 0, 1, 3),
-    ("rf", 1, 0, 1),
-    ("rf", 1, 0, 0),
-    ("rf", 1, 1, 1),
-    ("rd", 0, 1),
-    ("zr", 1, 1, 1),
-    ("zr", 1, 0, 3),
-    ("rd", 0, 2),
+    ("fx", 3),
+    ("ro", 0, 1),
+    ("rn", 1, 2),
+    ("sy", 0),
+    ("zr", 1, 1, 2),
+    ("rf", 1, 3, 0),
+    ("ro", 0, 3),
+    ("rf", 1, 3, 1),
+    ("rn", 1, 3),
+    ("ro", 0, 0),
+    ("ro", 1, 1),
     ("fx", 4),
-    ("zr", 1, 1, 2),
-    ("rf", 1, 1, 0),
-    ("rf", 1, 2, 0),
-    ("rf", 1, 2, 1),
-    ("rd", 0, 0),
-    ("sy", 0),
-    ("rd", 0, 3),
-    ("zr", 1, 1, 3),
-    ("rd", 1, 0),
-    ("rf", 1, 3, 1),
-    ("rf", 1, 3, 0),
-    ("fx", 1),
-    ("rd", 1, 1),
+    ("sy", 4),
+    ("ro", 0, 2),
+    ("ro", 1, 0),
+    ("ro", 1, 2),
+    ("sy", 3),
+    ("ro", 1, 3),
+    ("sy", 1),
     ("fx", 2),
-    ("rd", 1, 2),
-    ("sy", 4),
-    ("rd", 1, 3),
-    ("fx", 3),
-    ("sy", 1),
     ("sy", 2),
-    ("sy", 3),
 )
 REDUCE_ORDER = (
     ("pt", 0),
     ("pt", 1),
     ("op", 0),
-    ("g", 10),
     ("pt", 2),
+    ("g", 1),
     ("op", 1),
-    ("g", 6),
     ("pt", 3),
-    ("rl", 1, 1),
-    ("rl", 1, 0),
     ("rl", 0, 0),
+    ("rl", 2, 0),
     ("rl", 0, 1),
     ("op", 2),
+    ("to", 2, 0),
+    ("rl", 1, 1),
+    ("to", 0, 0),
+    ("rl", 3, 1),
     ("g", 8),
-    ("to", 1),
-    ("rl", 2, 0),
-    ("rl", 3, 1),
+    ("rl", 2, 1),
+    ("rl", 3, 0),
     ("rl", 4, 0),
-    ("rl", 3, 0),
+    ("rl", 4, 1),
+    ("rl", 1, 0),
+    ("to", 0, 1),
     ("g", 7),
-    ("rl", 2, 1),
-    ("rl", 4, 1),
+    ("g", 11),
+    ("g", 3),
+    ("rl", 5, 1),
+    ("rl", 5, 0),
+    ("mi", 2, 0),
     ("op", 3),
-    ("to", 0),
-    ("rl", 5, 1),
-    ("mi", 1),
-    ("to", 2),
-    ("to", 3),
-    ("to", 4),
-    ("mi", 0),
-    ("rl", 5, 0),
+    ("mi", 0, 0),
+    ("mi", 0, 1),
+    ("to", 1, 1),
+    ("to", 3, 1),
+    ("to", 3, 0),
+    ("g", 6),
+    ("to", 1, 0),
+    ("mi", 1, 1),
+    ("to", 2, 1),
+    ("to", 4, 1),
+    ("to", 5, 0),
+    ("g", 4),
+    ("mi", 3, 1),
+    ("to", 4, 0),
+    ("rl", 6, 1),
     ("rl", 6, 0),
-    ("rl", 6, 1),
-    ("lt", 1),
+    ("g", 9),
+    ("g", 5),
+    ("lt", 0, 0),
+    ("mi", 3, 0),
+    ("rl", 7, 0),
+    ("to", 5, 1),
     ("rl", 7, 1),
-    ("rl", 7, 0),
-    ("mi", 2),
-    ("mi", 3),
-    ("to", 5),
-    ("g", 0),
-    ("to", 6),
-    ("to", 7),
-    ("lt", 0),
-    ("mi", 4),
-    ("lt", 2),
-    ("g", 11),
+    ("mi", 1, 0),
+    ("lt", 1, 1),
+    ("to", 6, 1),
+    ("lt", 0, 1),
+    ("to", 6, 0),
+    ("mi", 2, 1),
+    ("mi", 4, 1),
+    ("lt", 3, 1),
+    ("mi", 4, 0),
+    ("to", 7, 0),
+    ("to", 7, 1),
+    ("mi", 5, 0),
     ("gd", 0),
-    ("lt", 3),
-    ("mi", 5),
+    ("lt", 1, 0),
+    ("lt", 3, 0),
+    ("lt", 2, 0),
     ("gd", 1),
     ("pj", 0),
+    ("mi", 5, 1),
+    ("lt", 4, 1),
+    ("lt", 2, 1),
+    ("mi", 6, 1),
+    ("lt", 4, 0),
     ("gd", 2),
-    ("g", 5),
-    ("lt", 4),
     ("gd", 3),
-    ("mi", 6),
-    ("g", 3),
-    ("mi", 7),
+    ("mi", 6, 0),
+    ("lt", 5, 0),
     ("pj", 1),
-    ("lt", 5),
+    ("mi", 7, 0),
+    ("g", 10),
+    ("lt", 5, 1),
+    ("mi", 7, 1),
     ("gd", 4),
-    ("g", 1),
-    ("lt", 6),
+    ("g", 0),
+    ("lt", 6, 1),
     ("gd", 5),
-    ("g", 4),
     ("pj", 2),
-    ("lt", 7),
+    ("lt", 6, 0),
+    ("lt", 7, 0),
+    ("lt", 7, 1),
     ("gd", 6),
-    ("g", 2),
     ("gd", 7),
     ("mb",),
+    ("mb2",),
     ("pj", 3),
-    ("mb2",),
-    ("g", 9),
+    ("g", 2),
     ("mb3",),
     ("mf",),
 )
@@ -457,9 +491,11 @@
 
 
 def layer_kernel(
-    x_ref, cot_ref, small_ref, gate_ref, up_ref, down_ref, out_ref,
-    query_ref, key_ref, value_ref, logit_ref,
+    x_far, cot_far, ids_far, probs_far, group_far, gate_far, up_far, down_far, out_far,
+    query_far, key_far, value_far, logit_far,
     gate_out, up_out, down_out, proj_out, query_out, key_out, value_out, logit_out,
+    x_ref, cot_ref, ids_ref, probs_ref, group_ref, gate_ref, up_ref, down_ref, out_ref,
+    query_ref, key_ref, value_ref, logit_ref, load_sem,
     mixed, small_buf, small_out, state_buf, state_out, future_buf, future_out,
     decayed, key_back, key_end, state_own, entry, span_end, scores, mixer_out, mixer_cot,
     proj_to, proj_from, summed, terms, weights,
@@ -469,11 +505,24 @@
     fs, fr, js, jr, bs, br, r1s, r1r, r2s, r2r, zts, ztr, ms, mr,
 ):
     here = Place()
+    loads = [
+        pltpu.make_async_copy(far, near, load_sem.at[i])
+        for i, (far, near) in enumerate((
+            (x_far, x_ref), (cot_far, cot_ref), (ids_far, ids_ref), (probs_far, probs_ref),
+            (group_far, group_ref), (query_far, query_ref), (key_far, key_ref),
+            (value_far, value_ref), (logit_far, logit_ref), (gate_far, gate_ref),
+            (up_far, up_ref), (down_far, down_ref), (out_far, out_ref),
+        ))
+    ]
+    for copy in loads:
+        copy.start()
     tok_rows, width = x_ref.shape
     lead = tok_rows * 4 // EXPERT_CUT
     tail = tok_rows - lead
     ins, alls = (x_ref, cot_ref), (x_all, cot_all)
     greet([here.right, here.across, here.left, here.near, here.far, here.pair])
+    for copy in loads[:2]:
+        copy.wait()
     plain, guarded = [], []
 
     def go(source, target, send_sem, recv_sem, device):
@@ -556,15 +605,20 @@
         arrived(pr.at[a, n, 3 * h], region)
         go(region, region, ps.at[a, n, 4 + h], pr.at[a, n, 4 + h], (here.right, here.left)[h])
 
-    def ring_finish(a, unit):
+    def ring_near(a, unit):
         n = number(unit)
         arrived(pr.at[a, n, 1], ring_region(a, unit, 3, 1))
         arrived(pr.at[a, n, 2], ring_region(a, unit, 1, 0))
+        if unit[1] == 0:
+            pair_send(a, unit[0], 1)
+            pair_send(a, unit[0], 3)
+
+    def ring_across(a, unit):
+        n = number(unit)
         arrived(pr.at[a, n, 4], ring_region(a, unit, 2, 0))
         arrived(pr.at[a, n, 5], ring_region(a, unit, 2, 1))
         if unit[1] == 0:
-            for step in (1, 3, 2):
-                pair_send(a, unit[0], step)
+            pair_send(a, unit[0], 2)
         else:
             z_start(a, 1)
             region = piece(a, 1, 0)
@@ -630,6 +684,8 @@
         )
 
     def mix_prepare():
+        for copy in loads[2:]:
+            copy.wait()
         ones = triangle().astype(bf16)
         high, low = two(log_decay(logit_ref[...].astype(f32)))
         cumulative = dot(ones, high) + dot(ones, low)
@@ -645,7 +701,13 @@
         state = join([dot(ends, value_ref[:, head_cols(h)], 0, 0) for h in range(heads)], row)
         state_own[...] = state
         state_buf[...] = state.astype(bf16)
-        small_buf[:, pl.ds(0, tok_rows)] = small_ref[...]
+        share = group_ref[...].reshape(1, tok_rows) / (probs_ref[0:1, :] + probs_ref[1:2, :])
+        expert = lax.broadcasted_iota(jnp.int32, (small_buf.shape[0], tok_rows), 0)
+        small_buf[...] = jnp.zeros_like(small_buf)
+        small_buf[:, pl.ds(0, tok_rows)] = sum(
+            jnp.where(ids_ref[j : j + 1, :] == expert, share * probs_ref[j : j + 1, :], 0.0)
+            for j in range(2)
+        )
         small_buf[RING : RING + 1, pl.ds(0, key_cols)] = jnp.exp(last)
         small_out[here.sp] = small_buf[...]
         state_out[here.sp] = state_buf[...]
@@ -786,7 +848,8 @@
         "rs": lambda a, n: own_start(a) if n == 0 else ring_send(a, (0, 1)),
         "zr": z_relay,
         "rf": lambda a, n, h: ring_forward(a, (n % 4, n // 4), h),
-        "rd": lambda a, n: ring_finish(a, (n % 4, n // 4)),
+        "rn": lambda a, n: ring_near(a, (n % 4, n // 4)),
+        "ro": lambda a, n: ring_across(a, (n % 4, n // 4)),
         "prep": mix_prepare,
         "mixf": mix_forward,
         "fx": lambda i: rows_of(0, i, forward_rows),
@@ -859,41 +922,54 @@
             r2s.at[k, 2 + h], r2r.at[k, 2 + h], device,
         )
 
-    def ring_total(k):
-        arrived(r2r.at[k, 0], second_in.at[k, 0, bottom])
-        arrived(r2r.at[k, 1], second_in.at[k, 1, top])
-        arrived(r2r.at[k, 2], second_in.at[k, 0, top])
-        arrived(r2r.at[k, 3], second_in.at[k, 1, bottom])
-        total[k] = (
-            parts[k, here.sp].astype(jnp.float32)
-            + second_in[k, 0].astype(jnp.float32)
-            + second_in[k, 1].astype(jnp.float32)
+    halves = (top, bottom)
+
+    def ring_total(k, h):
+        rows = halves[h]
+        own_sem, sum_sem = ((1, 2), (0, 3))[h]
+        own_from, sum_from = ((1, 0), (0, 1))[h]
+        arrived(r2r.at[k, own_sem], second_in.at[k, own_from, rows])
+        arrived(r2r.at[k, sum_sem], second_in.at[k, sum_from, rows])
+        total[k, rows] = (
+            parts[k, here.sp, rows].astype(jnp.float32)
+            + second_in[k, 0, rows].astype(jnp.float32)
+            + second_in[k, 1, rows].astype(jnp.float32)
         ).astype(jnp.bfloat16)
-        go_if(here.end, total.at[k], z_in.at[k, 0], zts.at[k, 0], ztr.at[k, 0], here.near)
-
-    def line_middle(k):
-        copy = remote(half_total.at[k], z_in.at[k, 1], zts.at[k, 1], ztr.at[k, 1], here.far)
+        go_if(
+            here.end, total.at[k, rows], z_in.at[k, 0, rows], zts.at[k, h, 0], ztr.at[k, h, 0],
+            here.near,
+        )
+
+    def line_middle(k, h):
+        rows = halves[h]
+        copy = remote(
+            half_total.at[k, rows], z_in.at[k, 1, rows], zts.at[k, h, 1], ztr.at[k, h, 1], here.far
+        )
 
         @pl.when(here.inner)
         def _():
-            arrived(ztr.at[k, 0], z_in.at[k, 0])
-            half_total[k] = (
-                total[k].astype(jnp.float32) + z_in[k, 0].astype(jnp.float32)
+            arrived(ztr.at[k, h, 0], z_in.at[k, 0, rows])
+            half_total[k, rows] = (
+                total[k, rows].astype(jnp.float32) + z_in[k, 0, rows].astype(jnp.float32)
             ).astype(jnp.bfloat16)
             copy.start()
 
         guarded.append((here.inner, copy))
 
-    def line_total(k):
-        region = mixed.at[k, here.core]
-        copy = remote(region, region, ms.at[k, 0], mr.at[k, 0], here.near)
+    def line_total(k, h):
+        rows = halves[h]
+        region = mixed.at[k, here.core, rows]
+        copy = remote(region, region, ms.at[k, h, 0], mr.at[k, h, 0], here.near)
 
         @pl.when(here.inner)
         def _():
-            arrived(ztr.at[k, 1], z_in.at[k, 1])
-            mixed[k, here.core] = (
-                columns(cot_all.at[here.sp], k, here.core).astype(jnp.float32)
-                + (half_total[k].astype(jnp.float32) + z_in[k, 1].astype(jnp.float32))
+            arrived(ztr.at[k, h, 1], z_in.at[k, 1, rows])
+            mixed[k, here.core, rows] = (
+                columns(cot_all.at[here.sp, rows], k, here.core).astype(jnp.float32)
+                + (
+                    half_total[k, rows].astype(jnp.float32)
+                    + z_in[k, 1, rows].astype(jnp.float32)
+                )
             ).astype(jnp.bfloat16)
             copy.start()
 
@@ -901,9 +977,9 @@
 
         @pl.when(here.end)
         def _():
-            arrived(mr.at[k, 0], region)
-
-        go(region, region, ms.at[k, 1], mr.at[k, 1], here.pair)
+            arrived(mr.at[k, h, 0], region)
+
+        go(region, region, ms.at[k, h, 1], mr.at[k, h, 1], here.pair)
 
     features = gate_ref.shape[1]
     block_cols = 2 * width
@@ -925,7 +1001,8 @@
         )
 
     def group_done(k):
-        arrived(mr.at[k, 1], mixed.at[k, 1 - here.core])
+        for h in range(2):
+            arrived(mr.at[k, h, 1], mixed.at[k, 1 - here.core, halves[h]])
         if (k + 1) % per:
             return
         m = k // per
@@ -972,7 +1049,8 @@
             copy.wait_send()
 
 
-def layer_stage(x, cot, small, gate, up, down, out_weight, query, key_in, value, logit):
+def layer_stage(*inputs):
+    x, _, _, _, _, gate, _, _, _, query, key_in, value, logit = inputs
     tok_rows, width = x.shape
     hidden_dev, features = gate.shape
     key_cols, value_cols = query.shape[1], value.shape[1]
@@ -987,16 +1065,17 @@
     block = (tok_rows, wide)
     state = (key_cols, DV)
     proj = (RING, RING, features // RING**2, value_cols)
-    table = (small.shape[0], -(-max(tok_rows, key_cols) // 128) * 128)
+    table = (8, -(-max(tok_rows, key_cols) // 128) * 128)
     results = [(hidden_dev, features)] * 3 + [
         (features // RING, value_cols), query.shape, key_in.shape, value.shape, logit.shape
     ]
     return pl.pallas_call(
         layer_kernel,
         out_shape=[jax.ShapeDtypeStruct(shape, f32) for shape in results],
-        in_specs=[vmem] * 11,
+        in_specs=[pl.BlockSpec(memory_space=pltpu.HBM)] * 13,
         out_specs=[vmem] * 8,
-        scratch_shapes=[
+        scratch_shapes=[pltpu.VMEM(a.shape, a.dtype) for a in inputs] + [
+            dma((len(inputs),)),
             pltpu.VMEM((pieces, 2) + block, bf16),
             pltpu.VMEM(table, f32), pltpu.VMEM((RING,) + table, f32),
             pltpu.VMEM(state, bf16), pltpu.VMEM((RING,) + state, bf16),
@@ -1026,14 +1105,14 @@
             dma((pieces,)), dma((pieces,)),
             dma((pieces, 2)), dma((pieces, 2)),
             dma((pieces, 4)), dma((pieces, 4)),
-            dma((pieces, 2)), dma((pieces, 2)),
-            dma((pieces, 2)), dma((pieces, 2)),
+            dma((pieces, 2, 2)), dma((pieces, 2, 2)),
+            dma((pieces, 2, 2)), dma((pieces, 2, 2)),
         ],
         compiler_params=pltpu.CompilerParams(
-            collective_id=0, has_side_effects=True, vmem_limit_bytes=60 << 20
+            collective_id=0, has_side_effects=True, vmem_limit_bytes=42 << 20
         ),
         name="layer_stage",
-    )(x, cot, small, gate, up, down, out_weight, query, key_in, value, logit)
+    )(*[pltpu.with_memory_space_constraint(a, pltpu.HBM) for a in inputs])
 
 
 def write_kernel(*refs):
@@ -1055,6 +1134,7 @@
         in_specs=[pl.BlockSpec(memory_space=pltpu.VMEM)] * len(arrays),
         out_specs=[pl.BlockSpec(memory_space=pltpu.HBM)] * len(arrays),
         scratch_shapes=[pltpu.SemaphoreType.DMA((len(arrays),))],
+        compiler_params=pltpu.CompilerParams(vmem_limit_bytes=1 << 20),
         name="write_out",
     )(*arrays)
 
@@ -1063,16 +1143,8 @@
     layer_in, out_cot, route_ids, route_probs, group_prob, gate_weight, up_weight,
     down_weight, out_weight, query, key_in, value, decay_logit,
 ):
-    total = route_probs[:, 0] + route_probs[:, 1]
-    expert = jnp.arange(8, dtype=jnp.int32)[:, None]
-    small = sum(
-        jnp.where(
-            route_ids[:, j][None] == expert, (group_prob * route_probs[:, j] / total)[None], 0.0
-        )
-        for j in range(2)
-    )
     results = write_out(layer_stage(
-        layer_in, out_cot, small, gate_weight[0], up_weight[0], down_weight[0],
+        layer_in, out_cot, route_ids.T, route_probs.T, group_prob, gate_weight[0], up_weight[0], down_weight[0],
         out_weight, query, key_in, value, decay_logit,
     ))
     return tuple(r[None] for r in results[:3]) + tuple(results[3:])

time: 117 us -> 105 us (0.90)
  Pallas kernels: 113 us -> 104 us
  local copies, waits for them, and re-layouts: 1.56 us -> 0 us
  other arithmetic: 1.3 us -> 0 us
    pallas_call x1, Pallas kernels: 107 us -> 101 us  [layer_stage(): pl.pallas_call(layer_kernel, out_shape=[jax.ShapeDtypeStruct(shape, f32)...]
    pallas_call x1, Pallas kernels: 6.23 us -> 3.11 us  [write_out(): pl.pallas_call(write_kernel, out_shape=[jax.ShapeDtypeStruct(a.shape, a.d...]
    slice x2 -> x0, local copies, waits for them, and re-layouts: 1.56 us -> none  [the longest x1 0.78 us: ring_local(): route_probs[:, j]]
where the time goes in v3:
time: 105 us
  Pallas kernels  104 us (99%)
    pallas_call x1, Pallas kernels, layer_stage(): pl.pallas_call(layer_kernel, out_shape=[jax.ShapeDtypeStruct(shape, f32)...  101 us
    pallas_call x1, Pallas kernels, write_out(): pl.pallas_call(write_kernel, out_shape=[jax.ShapeDtypeStruct(a.shape, a.d...  3.11 us

profile of v3, /device:TPU:0, one launch (start us, length us, event | category | flops | bytes accessed | tf_op | source)
XLA Modules:
  0.0 104.8 jit_solution(652684537815633751)
XLA Ops:
  0.6 100.9 %layer_stage.1 = (f32[256,2048]{1,0:T(8,128)S(1)}, f32[256,2048]{1,0:T(8,128)S(1)}, f32[256,2048]{1,0:T(8,128)S(1)}, f32[512,256]{1,0:T(8,128)S(1)}, f32[320,128...) custom-call(bf16[320,256]{1,0:T(8,128)(2,1)} %x_far.1, ...), custom_call_target="tpu_custom_call" | custom-call | tf_op jit(solution)/shard_map/layer_stage/pallas_call | solution.py:1072
  101.5 3.1 %write_out.1 = (f32[256,2048]{1,0:T(8,128)}, f32[256,2048]{1,0:T(8,128)}, f32[256,2048]{1,0:T(8,128)}, f32[512,256]{1,0:T(8,128)}, f32[320,128]{1,0:T(8,128)}, /...) custom-call(f32[256,2048]{1,0:T(8,128)S(1)} %get-tuple-element.24.refs_0_, ...), custom_call_target="tpu_custom_call" | custom-call | tf_op jit(solution)/shard_map/write_out/pallas_call | solution.py:1131

commit v4 on v3

--- a/solution.py
+++ b/solution.py
@@ -323,122 +323,126 @@
     ("rn", 1, 2),
     ("sy", 0),
     ("zr", 1, 1, 2),
+    ("fx", 4),
+    ("ro", 0, 3),
+    ("ro", 0, 0),
     ("rf", 1, 3, 0),
-    ("ro", 0, 3),
     ("rf", 1, 3, 1),
+    ("ro", 0, 2),
+    ("fx", 2),
     ("rn", 1, 3),
-    ("ro", 0, 0),
+    ("sy", 4),
     ("ro", 1, 1),
-    ("fx", 4),
-    ("sy", 4),
-    ("ro", 0, 2),
     ("ro", 1, 0),
     ("ro", 1, 2),
     ("sy", 3),
-    ("ro", 1, 3),
     ("sy", 1),
-    ("fx", 2),
-    ("sy", 2),
 )
 REDUCE_ORDER = (
-    ("pt", 0),
-    ("pt", 1),
-    ("op", 0),
+    ("ptb", 0),
+    ("ro", 1, 3),
+    ("sy", 2),
+    ("pto", 0),
+    ("opb", 0),
+    ("g", 11),
+    ("pto", 1),
+    ("ptb", 1),
+    ("opo", 0),
     ("pt", 2),
+    ("opo", 1),
+    ("opb", 1),
+    ("rl", 0, 1),
+    ("rl", 2, 0),
+    ("rl", 1, 0),
+    ("rl", 1, 1),
+    ("rl", 2, 1),
+    ("op", 2),
+    ("g", 6),
+    ("pt", 3),
+    ("to", 2, 0),
+    ("to", 1, 0),
+    ("g", 7),
+    ("to", 1, 1),
+    ("g", 9),
+    ("rl", 4, 0),
+    ("rl", 3, 1),
+    ("g", 0),
+    ("rl", 0, 0),
+    ("rl", 4, 1),
     ("g", 1),
-    ("op", 1),
-    ("pt", 3),
-    ("rl", 0, 0),
-    ("rl", 2, 0),
-    ("rl", 0, 1),
-    ("op", 2),
-    ("to", 2, 0),
-    ("rl", 1, 1),
+    ("to", 0, 1),
+    ("rl", 5, 0),
+    ("mi", 1, 0),
+    ("rl", 3, 0),
+    ("mi", 2, 0),
+    ("to", 2, 1),
+    ("rl", 5, 1),
+    ("op", 3),
+    ("to", 4, 0),
+    ("mi", 0, 1),
     ("to", 0, 0),
-    ("rl", 3, 1),
-    ("g", 8),
-    ("rl", 2, 1),
-    ("rl", 3, 0),
-    ("rl", 4, 0),
-    ("rl", 4, 1),
-    ("rl", 1, 0),
-    ("to", 0, 1),
-    ("g", 7),
-    ("g", 11),
-    ("g", 3),
-    ("rl", 5, 1),
-    ("rl", 5, 0),
-    ("mi", 2, 0),
-    ("op", 3),
+    ("mi", 1, 1),
+    ("to", 3, 1),
+    ("to", 5, 0),
+    ("lt", 1, 0),
+    ("to", 3, 0),
+    ("g", 10),
+    ("rl", 6, 1),
+    ("mi", 4, 0),
+    ("rl", 6, 0),
+    ("to", 4, 1),
+    ("lt", 2, 0),
+    ("mi", 2, 1),
     ("mi", 0, 0),
-    ("mi", 0, 1),
-    ("to", 1, 1),
-    ("to", 3, 1),
-    ("to", 3, 0),
-    ("g", 6),
-    ("to", 1, 0),
-    ("mi", 1, 1),
-    ("to", 2, 1),
-    ("to", 4, 1),
-    ("to", 5, 0),
-    ("g", 4),
-    ("mi", 3, 1),
-    ("to", 4, 0),
-    ("rl", 6, 1),
-    ("rl", 6, 0),
-    ("g", 9),
     ("g", 5),
-    ("lt", 0, 0),
-    ("mi", 3, 0),
-    ("rl", 7, 0),
     ("to", 5, 1),
     ("rl", 7, 1),
-    ("mi", 1, 0),
+    ("lt", 0, 1),
+    ("mi", 3, 1),
+    ("rl", 7, 0),
+    ("g", 3),
+    ("to", 6, 1),
+    ("to", 6, 0),
     ("lt", 1, 1),
-    ("to", 6, 1),
-    ("lt", 0, 1),
-    ("to", 6, 0),
-    ("mi", 2, 1),
+    ("g", 2),
+    ("mi", 3, 0),
+    ("lt", 4, 0),
     ("mi", 4, 1),
+    ("to", 7, 1),
+    ("to", 7, 0),
+    ("lt", 0, 0),
+    ("lt", 2, 1),
+    ("mi", 5, 0),
     ("lt", 3, 1),
-    ("mi", 4, 0),
-    ("to", 7, 0),
-    ("to", 7, 1),
-    ("mi", 5, 0),
     ("gd", 0),
-    ("lt", 1, 0),
+    ("gd", 1),
+    ("mi", 5, 1),
+    ("pj", 0),
+    ("gd", 2),
     ("lt", 3, 0),
-    ("lt", 2, 0),
-    ("gd", 1),
-    ("pj", 0),
-    ("mi", 5, 1),
+    ("mi", 6, 1),
     ("lt", 4, 1),
-    ("lt", 2, 1),
-    ("mi", 6, 1),
-    ("lt", 4, 0),
-    ("gd", 2),
+    ("mi", 6, 0),
     ("gd", 3),
-    ("mi", 6, 0),
+    ("gd", 4),
     ("lt", 5, 0),
     ("pj", 1),
-    ("mi", 7, 0),
-    ("g", 10),
     ("lt", 5, 1),
     ("mi", 7, 1),
-    ("gd", 4),
-    ("g", 0),
+    ("mi", 7, 0),
     ("lt", 6, 1),
     ("gd", 5),
+    ("g", 8),
+    ("lt", 6, 0),
     ("pj", 2),
-    ("lt", 6, 0),
+    ("lt", 7, 1),
     ("lt", 7, 0),
-    ("lt", 7, 1),
     ("gd", 6),
     ("gd", 7),
     ("mb",),
+    ("pj", 3),
+    ("g", 4),
     ("mb2",),
-    ("pj", 3),
-    ("g", 2),
     ("mb3",),
     ("mf",),
 )
@@ -857,9 +861,6 @@
     }
     for a in range(2):
         alls[a][here.sp, :, cols(0, here.core)] = ins[a][...]
-    for name, *rest in GATHER_ORDER:
-        gather_steps[name](*rest)
-
     pieces, wide = parts.shape[0], parts.shape[3]
     split = tok_rows // 2
     span = gate_ref.shape[1] // RING
@@ -876,38 +877,61 @@
 
     top, bottom = pl.ds(0, split), pl.ds(split, split)
 
-    def partial(m, core):
-        rows = RING * tok_rows
-        total_of = [
-            jnp.dot(
-                cot[...].reshape(rows, width),
-                jnp.concatenate([columns(ref, m * per + i, core) for i in range(per)], axis=1),
-                preferred_element_type=jnp.float32,
+    def partial(m, core, steps):
+        weight_of = [
+            jnp.concatenate([columns(ref, m * per + i, core) for i in range(per)], axis=1)
+            for ref in (gate_ref, up_ref)
+        ]
+        sides = (gate_cot, up_cot)
+        if len(steps) == RING:
+            rows = RING * tok_rows
+            both = sum(
+                jnp.dot(c[...].reshape(rows, width), w, preferred_element_type=jnp.float32)
+                for c, w in zip(sides, weight_of)
             )
-            for cot, ref in ((gate_cot, gate_ref), (up_cot, up_ref))
-        ]
-        both = total_of[0] + total_of[1]
-        for i in range(per):
-            part = both[:, i * wide : (i + 1) * wide]
-            yield m * per + i, part.reshape(RING, tok_rows, wide)
-
-    def pair_part(m):
-        for k, part in partial(m, 1 - here.core):
-            pair_to[k] = part.astype(jnp.bfloat16)
-            go(pair_to.at[k], pair_from.at[k], bs.at[k], br.at[k], here.pair)
-
-    def own_part(m):
-        for k, part in partial(m, here.core):
-            arrived(br.at[k], pair_from.at[k])
-            parts[k] = (part + pair_from[k].astype(jnp.float32)).astype(jnp.bfloat16)
+            for i in range(per):
+                part = both[:, i * wide : (i + 1) * wide]
+                yield m * per + i, slice(None), part.reshape(RING, tok_rows, wide)
+            return
+        for step in steps:
+            s = here.at[step]
+            both = sum(
+                jnp.dot(c[s], w, preferred_element_type=jnp.float32)
+                for c, w in zip(sides, weight_of)
+            )
+            for i in range(per):
+                yield m * per + i, s, both[:, i * wide : (i + 1) * wide]
+
+    everything, beside, others = (2, 1, 3, 0), (1, 3), (2, 0)
+
+    def pair_part(m, steps):
+        for k, s, part in partial(m, 1 - here.core, steps):
+            pair_to[k, s] = part.astype(jnp.bfloat16)
+        for k in range(m * per, (m + 1) * per):
+            for step in steps:
+                s = here.at[step]
+                go(
+                    pair_to.at[k, s], pair_from.at[k, s], bs.at[k, step], br.at[k, step], here.pair
+                )
+
+    def own_part(m, steps):
+        for k in range(m * per, (m + 1) * per):
+            for step in steps:
+                arrived(br.at[k, step], pair_from.at[k, here.at[step]])
+        for k, s, part in partial(m, here.core, steps):
+            parts[k, s] = (part + pair_from[k, s].astype(jnp.float32)).astype(jnp.bfloat16)
+        for k in range(m * per, (m + 1) * per):
             right, across, left = [parts.at[k, here.at[i]] for i in (1, 2, 3)]
-            go(across.at[top], first_in.at[k, 0], r1s.at[k, 0], r1r.at[k, 0], here.right)
-            go(across.at[bottom], first_in.at[k, 1], r1s.at[k, 1], r1r.at[k, 1], here.left)
-            go(
-                right.at[bottom], second_in.at[k, 0, bottom], r2s.at[k, 0], r2r.at[k, 0],
-                here.right,
-            )
-            go(left.at[top], second_in.at[k, 1, top], r2s.at[k, 1], r2r.at[k, 1], here.left)
+            if 2 in steps:
+                go(across.at[top], first_in.at[k, 0], r1s.at[k, 0], r1r.at[k, 0], here.right)
+                go(across.at[bottom], first_in.at[k, 1], r1s.at[k, 1], r1r.at[k, 1], here.left)
+            if 1 in steps:
+                go(
+                    right.at[bottom], second_in.at[k, 0, bottom], r2s.at[k, 0], r2r.at[k, 0],
+                    here.right,
+                )
+            if 3 in steps:
+                go(left.at[top], second_in.at[k, 1, top], r2s.at[k, 1], r2r.at[k, 1], here.left)
 
     def add_to(ref, other):
         ref[...] = (ref[...].astype(jnp.float32) + other.astype(jnp.float32)).astype(jnp.bfloat16)
@@ -1025,8 +1049,12 @@
             )
 
     reduce_steps = {
-        "pt": pair_part,
-        "op": own_part,
+        "pt": lambda m: pair_part(m, everything),
+        "op": lambda m: own_part(m, everything),
+        "ptb": lambda m: pair_part(m, beside),
+        "opb": lambda m: own_part(m, beside),
+        "pto": lambda m: pair_part(m, others),
+        "opo": lambda m: own_part(m, others),
         "g": weight_grad,
         "rl": ring_relay,
         "to": ring_total,
@@ -1039,8 +1067,9 @@
         "mb3": mix_outer,
         "mf": mix_finish,
     }
-    for name, *rest in REDUCE_ORDER:
-        reduce_steps[name](*rest)
+    steps = {**gather_steps, **reduce_steps}
+    for name, *rest in GATHER_ORDER + REDUCE_ORDER:
+        steps[name](*rest)
     for copy in plain:
         copy.wait_send()
     for cond, copy in guarded:
@@ -1102,7 +1131,7 @@
             dma((2, 5, 6)), dma((2, 5, 6)),
             dma((2, 4, 5)), dma((2, 4, 5)),
             dma((3,)), dma((3,)), dma((RING, 3)), dma((RING, 3)),
-            dma((pieces,)), dma((pieces,)),
+            dma((pieces, RING)), dma((pieces, RING)),
             dma((pieces, 2)), dma((pieces, 2)),
             dma((pieces, 4)), dma((pieces, 4)),
             dma((pieces, 2, 2)), dma((pieces, 2, 2)),

time: 105 us -> 104 us (level)
  no operation moved by 1% of the time
where the time goes in v4:
time: 104 us
  Pallas kernels  103 us (99%)
    pallas_call x1, Pallas kernels, layer_stage(): pl.pallas_call(layer_kernel, out_shape=[jax.ShapeDtypeStruct(shape, f32)...  100 us
    pallas_call x1, Pallas kernels, write_out(): pl.pallas_call(write_kernel, out_shape=[jax.ShapeDtypeStruct(a.shape, a.d...  3.11 us

profile of v4, /device:TPU:0, one launch (start us, length us, event | category | flops | bytes accessed | tf_op | source)
XLA Modules:
  0.0 104.2 jit_solution(11116201320933923506)
XLA Ops:
  0.6 100.3 %layer_stage.1 = (f32[256,2048]{1,0:T(8,128)S(1)}, f32[256,2048]{1,0:T(8,128)S(1)}, f32[256,2048]{1,0:T(8,128)S(1)}, f32[512,256]{1,0:T(8,128)S(1)}, f32[320,128...) custom-call(bf16[320,256]{1,0:T(8,128)(2,1)} %x_far.1, ...), custom_call_target="tpu_custom_call" | custom-call | tf_op jit(solution)/shard_map/layer_stage/pallas_call | solution.py:1101
  101.0 3.1 %write_out.1 = (f32[256,2048]{1,0:T(8,128)}, f32[256,2048]{1,0:T(8,128)}, f32[256,2048]{1,0:T(8,128)}, f32[512,256]{1,0:T(8,128)}, f32[320,128]{1,0:T(8,128)}, /...) custom-call(f32[256,2048]{1,0:T(8,128)S(1)} %get-tuple-element.24.refs_0_, ...), custom_call_target="tpu_custom_call" | custom-call | tf_op jit(solution)/shard_map/write_out/pallas_call | solution.py:1160
